TPU v7x, 32 devices: a whole 2x2x4 slice. The times are simulated.
32 devices in a mesh: grp: 2 (over y), sp: 4 (over z), tp: 4 (over x, core).
Axes of the slice: x: 2, y: 2, z: 4, core: 2. Of those that a mesh axis runs over, the one named last changes fastest.
Arguments:
- source: bfloat16 [4096, 2048], P(('grp', 'sp', 'tp')), parts along dimension 0, may hold values from -8 to 8
- target: bfloat16 [1024, 2048], P(('grp', 'sp', 'tp')), parts along dimension 0, may hold values from -8 to 8
- source_gain: float32 [2048], replicated, may hold values from 0.1 to 1.9
- attend_gain: float32 [2, 2048], replicated, may hold values from 0.1 to 1.9
- query_weight: bfloat16 [2, 2048, 2048], P(None, None, 'tp'), may hold values from -4 to 4
- key_weight: bfloat16 [2, 2048, 2048], P(None, None, 'tp'), may hold values from -4 to 4
- value_weight: bfloat16 [2, 2048, 2048], P(None, None, 'tp'), may hold values from -0.125 to 0.125
- out_weight: bfloat16 [2, 2048, 2048], P(None, 'tp'), may hold values from -3 to 3
- mixer_gain: float32 [2048], replicated, may hold values from 0.1 to 1.9
- gate_weight: bfloat16 [2048, 2816], P(None, 'tp'), may hold values from -0.125 to 0.125
- up_weight: bfloat16 [2048, 2816], P(None, 'tp'), may hold values from -0.125 to 0.125
- gate_taps: float32 [3, 2816], P(None, 'tp'), may hold values from -3 to 3
- up_taps: float32 [3, 2816], P(None, 'tp'), may hold values from -3 to 3
- down_weight: bfloat16 [2816, 2048], P('tp'), may hold values from -0.109375 to 0.109375
- final_gain: float32 [2048], replicated, may hold values from 0.1 to 1.9
Outputs:
- result: bfloat16 [1024, 2048], P(('grp', 'sp', 'tp')), parts along dimension 0
There are 2 independent parts, one for each index of `grp`. A program takes and returns all parts, laid end to end along the dimension named above; an argument that names none is the same for every part. Nothing has to cross between parts.
All inputs are finite; a program needn't handle non-finite values.
Results may differ from a plain program's by a relative error of at most 0.04.
Values may be sent and summed in bfloat16 or wider, within the bound.
A program may use at most 128 MiB of HBM per device.

v0:
```python
import functools

import jax
import jax.numpy as jnp
from jax import lax
from jax.experimental import pallas as pl
from jax.experimental.pallas import tpu as pltpu
from jax.sharding import PartitionSpec as P

HD = 256
EPS = 1e-06
TILE = 256
STAT_ROWS = 8
LANES = 128
MESH = pl.DeviceIdType.MESH
BF = jnp.bfloat16
F32 = jnp.float32


def normed_rows(wide, gain):
    return wide * lax.rsqrt(jnp.mean(wide * wide, axis=-1, keepdims=True) + EPS) * gain


def mm(a, b):
    return jnp.dot(a, b, preferred_element_type=F32)


def kernel(
    n,
    S,
    source,
    target,
    source_gain,
    attend_gain,
    query_weight,
    key_weight,
    value_weight,
    out_weight,
    mixer_gain,
    gate_weight,
    up_weight,
    gate_taps,
    up_taps,
    down_weight,
    final_gain,
    result,
    sv,
    tv,
    wq,
    wkv,
    wo,
    wg,
    wu,
    wd,
    xs,
    xt,
    kv,
    qall,
    osend,
    orecv,
    ssend,
    srecv,
    pf,
    att,
    p1s,
    p1r,
    p2s,
    p2r,
    hs,
    hr,
    gpad,
    upad,
    hid,
    residual,
    load_sem,
    w_sem,
    ag_send,
    ag_recv,
    q_send,
    q_recv,
    r_send,
    r_recv,
    s_send,
    s_recv,
    p1_send,
    p1_recv,
    p2_send,
    p2_recv,
    h_send,
    h_recv,
):
    X = n // 2
    Rs, D = source.shape
    Rt = target.shape[0]
    W = wq.shape[2]
    T = n * Rt
    heads = W // HD
    F = wg.shape[0]
    scale = HD ** (-0.5)
    t = lax.axis_index("tp")
    s = lax.axis_index("sp")
    x = lax.div(t, 2)
    c = lax.rem(t, 2)
    other = 1 - c
    peer = x * 2 + other
    pending = []

    def tp_at(k):
        return lax.rem(x + k, X)

    def tp_from(k):
        return lax.rem(x + X - k, X)

    def sp_at(i):
        return lax.rem(s + i, S)

    def remote(src, dst, ss, rs, axis, where):
        return pltpu.make_async_remote_copy(
            src_ref=src,
            dst_ref=dst,
            send_sem=ss,
            recv_sem=rs,
            device_id={axis: where},
            device_id_type=MESH,
        )

    def launch(copy):
        copy.start()
        pending.append(copy)

    barrier = pltpu.get_barrier_semaphore()
    pl.semaphore_signal(barrier, inc=1, device_id={"tp": peer}, device_id_type=MESH)
    for k in range(1, X):
        pl.semaphore_signal(
            barrier, inc=1, device_id={"tp": tp_at(k) * 2 + c}, device_id_type=MESH
        )
    for i in range(1, S):
        pl.semaphore_signal(barrier, inc=1, device_id={"sp": sp_at(i)}, device_id_type=MESH)

    load_t = pltpu.make_async_copy(target, tv, load_sem.at[0])
    load_s = pltpu.make_async_copy(source, sv, load_sem.at[1])
    load_t.start()
    load_s.start()
    load_q = [pltpu.make_async_copy(query_weight.at[l], wq.at[l], w_sem.at[l]) for l in range(2)]
    load_kv = []
    for l in range(2):
        load_kv.append(
            [
                pltpu.make_async_copy(key_weight.at[l], wkv.at[2 * l], w_sem.at[2 + 2 * l]),
                pltpu.make_async_copy(value_weight.at[l], wkv.at[2 * l + 1], w_sem.at[3 + 2 * l]),
            ]
        )
    load_o = [pltpu.make_async_copy(out_weight.at[l], wo.at[l], w_sem.at[6 + l]) for l in range(2)]
    load_m = [
        pltpu.make_async_copy(gate_weight, wg, w_sem.at[8]),
        pltpu.make_async_copy(up_weight, wu, w_sem.at[9]),
        pltpu.make_async_copy(down_weight, wd, w_sem.at[10]),
    ]
    load_q[0].start()

    def gather_start(a, buf):
        for k in range(1, X):
            launch(
                remote(
                    buf.at[t],
                    buf.at[t],
                    ag_send.at[a, k],
                    ag_recv.at[a, t],
                    "tp",
                    tp_at(k) * 2 + c,
                )
            )
        launch(remote(buf.at[t], buf.at[t], ag_send.at[a, 0], ag_recv.at[a, t], "tp", peer))

    def gather_wait(a, buf, slot):
        remote(
            buf.at[slot], buf.at[slot], ag_send.at[a, 0], ag_recv.at[a, slot], "tp", peer
        ).wait_recv()

    def gather_forward(a, buf):
        for k in range(1, X):
            slot = tp_from(k) * 2 + c
            gather_wait(a, buf, slot)
            launch(
                remote(
                    buf.at[slot],
                    buf.at[slot],
                    ag_send.at[a, X - 1 + k],
                    ag_recv.at[a, slot],
                    "tp",
                    peer,
                )
            )

    def gather_finish(a, buf):
        gather_forward(a, buf)
        for k in range(X):
            gather_wait(a, buf, tp_from(k) * 2 + other)

    def project_source(layer, at):
        rows = xs[pl.ds(2 * at, 2)].reshape(2 * Rs, D)

        def one(j, carry):
            kv[j, at] = mm(rows, wkv[j]).astype(BF)
            return carry

        lax.fori_loop(2 * layer, 2 * layer + 2, one, 0)

    def query_copy(layer, i, block, where):
        return remote(
            qall.at[layer, block],
            qall.at[layer, block],
            q_send.at[layer, i],
            q_recv.at[layer, block],
            "sp",
            where,
        )

    def send_queries(layer):
        load_q[layer].wait()
        rows = xt[layer].reshape(T, D)
        qall[layer, s] = mm(rows, wq[layer]).astype(BF)
        for i in range(1, S):
            launch(query_copy(layer, i, s, sp_at(i)))

    def attend_block(layer, block, sums, stats):
        lanes = lax.broadcasted_iota(jnp.int32, (T, LANES), 1)
        packed = jnp.zeros((T, LANES), F32)
        for h in range(heads):
            cols = slice(h * HD, (h + 1) * HD)
            query = qall[layer, block, :, cols]
            keys = kv[2 * layer, :, :, cols].reshape(n * Rs, HD)
            values = kv[2 * layer + 1, :, :, cols].reshape(n * Rs, HD)
            scores = (
                lax.dot_general(query, keys, (((1,), (1,)), ((), ())), preferred_element_type=F32)
                * scale
            )
            top = jnp.max(scores, axis=-1, keepdims=True)
            raised = jnp.exp(scores - top)
            total = jnp.sum(raised, axis=-1, keepdims=True)
            sums[:, cols] = mm(raised.astype(BF), values).astype(BF)
            packed = jnp.where(lanes == 2 * h, top, packed)
            packed = jnp.where(lanes == 2 * h + 1, total, packed)
        stats[...] = packed.T[:STAT_ROWS]

    def sums_copy(layer, i, slot, block):
        return remote(
            osend.at[layer, i],
            orecv.at[layer, slot],
            r_send.at[layer, i],
            r_recv.at[layer, slot],
            "sp",
            block,
        )

    def stats_copy(layer, i, slot, block):
        return remote(
            ssend.at[layer, i],
            srecv.at[layer, slot],
            s_send.at[layer, i],
            s_recv.at[layer, slot],
            "sp",
            block,
        )

    def attend(layer, meanwhile):
        attend_block(layer, s, orecv.at[layer, s], srecv.at[layer, s])

        def one(i, carry):
            block = sp_at(i)
            query_copy(layer, 0, block, block).wait_recv()
            attend_block(layer, block, osend.at[layer, block], ssend.at[layer, block])
            sums_copy(layer, block, s, block).start()
            stats_copy(layer, block, s, block).start()
            return carry

        lax.fori_loop(1, S, one, 0)
        meanwhile()

        def wait_block(i, carry):
            block = sp_at(i)
            sums_copy(layer, block, block, block).wait_recv()
            stats_copy(layer, block, block, block).wait_recv()
            return carry

        lax.fori_loop(1, S, wait_block, 0)
        rows = srecv[layer].reshape(S * STAT_ROWS, T)
        if S * STAT_ROWS < LANES:
            rows = jnp.concatenate([rows, jnp.zeros((LANES - S * STAT_ROWS, T), F32)], axis=0)
        stats = rows.T
        for h in range(heads):
            cols = slice(h * HD, (h + 1) * HD)
            tops = [stats[:, b * STAT_ROWS + 2 * h :][:, :1] for b in range(S)]
            highest = functools.reduce(jnp.maximum, tops)
            total = jnp.zeros((T, 1), F32)
            summed = jnp.zeros((T, HD), F32)
            for b in range(S):
                factor = jnp.exp(tops[b] - highest)
                total = total + factor * stats[:, b * STAT_ROWS + 2 * h + 1 :][:, :1]
                summed = summed + factor * orecv[layer, b, :, cols].astype(F32)
            att[:, cols] = (summed / total).astype(BF)
        load_o[layer].wait()
        spread_sum(layer, att, wo.at[layer])

    def spread_sum(a, lhs, weight):
        def one(j, carry):
            cols = pl.ds(pl.multiple_of(j * TILE, TILE), TILE)
            pf[:, :, cols] = mm(lhs[...], weight[:, cols]).reshape(n, Rt, TILE)
            return carry

        lax.fori_loop(0, D // TILE, one, 0)
        order = [*range(1, X), 0]

        def first(k):
            return remote(
                p1s.at[a, k], p1r.at[a, k], p1_send.at[a, k], p1_recv.at[a, k], "tp", peer
            )

        def second(k):
            return remote(
                p2s.at[a, k],
                p2r.at[a, k],
                p2_send.at[a, k],
                p2_recv.at[a, k],
                "tp",
                tp_at(k) * 2 + c,
            )

        for k in order:
            p1s[a, k] = pf[tp_at(k) * 2 + other].astype(BF)
            launch(first(k))
        for k in range(1, X):
            first(k).wait_recv()
            p2s[a, k] = (pf[tp_at(k) * 2 + c] + p1r[a, k].astype(F32)).astype(BF)
            launch(second(k))
        first(0).wait_recv()
        own = pf[t] + p1r[a, 0].astype(F32)
        for k in range(1, X):
            second(k).wait_recv()
            own = own + p2r[a, k].astype(F32)
        residual[...] = residual[...] + own

    load_t.wait()
    residual[...] = tv[...].astype(F32)
    xt[0, t] = normed_rows(residual[...], attend_gain[0:1]).astype(BF)
    pl.semaphore_wait(barrier, X + S - 1)
    gather_start(0, xt.at[0])
    for copy in load_kv[0]:
        copy.start()
    load_s.wait()
    step = 32

    def norm_source(j, carry):
        rows = pl.ds(pl.multiple_of(j * step, step), step)
        xs[t, rows] = normed_rows(sv[rows].astype(F32), source_gain[...]).astype(BF)
        return carry

    lax.fori_loop(0, Rs // step, norm_source, 0)
    gather_start(3, xs)
    gather_finish(0, xt.at[0])
    send_queries(0)
    for copy in [*load_kv[1], load_o[0], load_q[1], load_o[1]]:
        copy.start()
    for copy in load_kv[0]:
        copy.wait()
    gather_wait(3, xs, peer)
    project_source(0, x)
    for copy in load_kv[1]:
        copy.wait()
    project_source(1, x)
    for copy in load_m:
        copy.start()
    gather_forward(3, xs)
    for k in range(1, X):
        gather_wait(3, xs, tp_from(k) * 2 + other)
        project_source(0, tp_from(k))

    def rest_of_source():
        for k in range(1, X):
            project_source(1, tp_from(k))

    attend(0, rest_of_source)
    xt[1, t] = normed_rows(residual[...], attend_gain[1:2]).astype(BF)
    gather_start(1, xt.at[1])
    gather_finish(1, xt.at[1])
    send_queries(1)
    attend(1, lambda: None)
    xt[2, t] = normed_rows(residual[...], mixer_gain[...]).astype(BF)
    gather_start(2, xt.at[2])
    gather_finish(2, xt.at[2])
    load_m[0].wait()
    load_m[1].wait()
    mixed = xt[2].reshape(T, D)
    pads = ((gpad, wg), (upad, wu))

    def halo_out(number):
        return remote(
            hs.at[number],
            hr.at[number],
            h_send.at[number],
            h_recv.at[number],
            "sp",
            lax.rem(s + 1, S),
        )

    for number, (pad, weight) in enumerate(pads):
        lifted = (
            lax.dot_general(
                mixed, weight[...], (((1,), (1,)), ((), ())), preferred_element_type=F32
            )
            .astype(BF)
            .astype(F32)
        )
        hs[number] = lifted[T - 8 :]

        @pl.when(s < S - 1)
        def _():
            halo_out(number).start()

        pad[8:] = lifted

    def hidden_rows(start, stop):
        def convolved(pad, taps):
            return (
                taps[0:1] * pad[6 + start : 6 + stop]
                + taps[1:2] * pad[7 + start : 7 + stop]
                + taps[2:3] * pad[8 + start : 8 + stop]
            )

        gate = convolved(gpad, gate_taps)
        hid[start:stop] = (gate / (1.0 + jnp.exp(-gate)) * convolved(upad, up_taps)).astype(BF)

    hidden_rows(16, T)

    @pl.when(s == 0)
    def _():
        for pad, _weight in pads:
            pad[:8] = jnp.zeros((8, F), F32)

    @pl.when(s > 0)
    def _():
        for number, (pad, _weight) in enumerate(pads):
            halo_out(number).wait_recv()
            pad[:8] = hr[number]

    @pl.when(s < S - 1)
    def _():
        for number in range(2):
            halo_out(number).wait_send()

    hidden_rows(0, 16)
    load_m[2].wait()
    spread_sum(2, hid, wd)
    result[...] = normed_rows(residual[...], final_gain[...]).astype(BF)
    for copy in pending:
        copy.wait_send()
    for layer in range(2):

        def wait_sent(i, carry):
            block = sp_at(i)
            sums_copy(layer, block, s, block).wait_send()
            stats_copy(layer, block, s, block).wait_send()
            return carry

        lax.fori_loop(1, S, wait_sent, 0)


def body(n, S, *arrays):
    (
        source,
        target,
        source_gain,
        attend_gain,
        query_weight,
        key_weight,
        value_weight,
        out_weight,
        mixer_gain,
        gate_weight,
        up_weight,
        gate_taps,
        up_taps,
        down_weight,
        final_gain,
    ) = arrays
    Rs, D = source.shape
    Rt = target.shape[0]
    W = query_weight.shape[2]
    F = gate_weight.shape[1]
    T = n * Rt
    X = n // 2
    hbm = pl.BlockSpec(memory_space=pl.ANY)
    vmem = pl.BlockSpec(memory_space=pltpu.VMEM)
    dma = pltpu.SemaphoreType.DMA
    scratch = [
        pltpu.VMEM((Rs, D), BF),
        pltpu.VMEM((Rt, D), BF),
        pltpu.VMEM((2, D, W), BF),
        pltpu.VMEM((4, D, W), BF),
        pltpu.VMEM((2, W, D), BF),
        pltpu.VMEM((F, D), BF),
        pltpu.VMEM((F, D), BF),
        pltpu.VMEM((F, D), BF),
        pltpu.VMEM((n, Rs, D), BF),
        pltpu.VMEM((3, n, Rt, D), BF),
        pltpu.VMEM((4, X, 2 * Rs, W), BF),
        pltpu.VMEM((2, S, T, W), BF),
        pltpu.VMEM((2, S, T, W), BF),
        pltpu.VMEM((2, S, T, W), BF),
        pltpu.VMEM((2, S, STAT_ROWS, T), F32),
        pltpu.VMEM((2, S, STAT_ROWS, T), F32),
        pltpu.VMEM((n, Rt, D), F32),
        pltpu.VMEM((T, W), BF),
        pltpu.VMEM((3, X, Rt, D), BF),
        pltpu.VMEM((3, X, Rt, D), BF),
        pltpu.VMEM((3, X, Rt, D), BF),
        pltpu.VMEM((3, X, Rt, D), BF),
        pltpu.VMEM((2, 8, F), F32),
        pltpu.VMEM((2, 8, F), F32),
        pltpu.VMEM((T + 8, F), F32),
        pltpu.VMEM((T + 8, F), F32),
        pltpu.VMEM((T, F), BF),
        pltpu.VMEM((Rt, D), F32),
        dma((2,)),
        dma((11,)),
        dma((4, n)),
        dma((4, n)),
        dma((2, S)),
        dma((2, S)),
        dma((2, S)),
        dma((2, S)),
        dma((2, S)),
        dma((2, S)),
        dma((3, X)),
        dma((3, X)),
        dma((3, X)),
        dma((3, X)),
        dma((2,)),
        dma((2,)),
    ]
    return pl.pallas_call(
        functools.partial(kernel, n, S),
        out_shape=jax.ShapeDtypeStruct((Rt, D), BF),
        in_specs=[
            hbm,
            hbm,
            vmem,
            vmem,
            hbm,
            hbm,
            hbm,
            hbm,
            vmem,
            hbm,
            hbm,
            vmem,
            vmem,
            hbm,
            vmem,
        ],
        out_specs=vmem,
        scratch_shapes=scratch,
        compiler_params=pltpu.CompilerParams(
            collective_id=0, has_side_effects=True, vmem_limit_bytes=67043328
        ),
    )(
        source,
        target,
        source_gain.reshape(1, D),
        attend_gain,
        query_weight,
        key_weight,
        value_weight,
        out_weight,
        mixer_gain.reshape(1, D),
        gate_weight.T,
        up_weight.T,
        gate_taps,
        up_taps,
        down_weight,
        final_gain.reshape(1, D),
    )


def solution(mesh):
    placed = (
        P(("grp", "sp", "tp"), None),
        P(("grp", "sp", "tp"), None),
        P(),
        P(),
        P(None, None, "tp"),
        P(None, None, "tp"),
        P(None, None, "tp"),
        P(None, "tp", None),
        P(),
        P(None, "tp"),
        P(None, "tp"),
        P(None, "tp"),
        P(None, "tp"),
        P("tp", None),
        P(),
    )
    return jax.shard_map(
        functools.partial(body, mesh.shape["tp"], mesh.shape["sp"]),
        mesh=mesh,
        in_specs=placed,
        out_specs=P(("grp", "sp", "tp"), None),
        check_vma=False,
    )
```

profile of v0, /device:TPU:0, one launch (start us, length us, event | category | flops | bytes accessed | tf_op | source)
XLA Modules:
  0.0 102.0 jit_solution(15526519098898153407)
XLA Ops:
  0.0 100.4 %shard_map.145 = bf16[32,2048]{1,0:T(8,128)(2,1)} custom-call(bf16[128,2048]{1,0:T(8,128)(2,1)} %source.1, bf16[32,2048]{1,0:T(8,128)(2,1)} %target.1, f32[1,2048]{1,0:T(1,128)} %bitcast.7, f32[2,2048]{1,0:T(2,128)} %attend_gain.1, bf16[2,2048,512]{2,1,0:T(8,128)(2,1)} %query_weight.1, bf16[2,2048,512]{2,1,0:T(8,128)(2,1)} %key_weight.1, ...), custom_call_target="tpu_custom_call" | custom-call | tf_op jit(solution)/shard_map/pallas_call | solution.py:541
  100.4 1.6 %copy.17 = bf16[32,2048]{1,0:T(8,128)(2,1)} copy(bf16[32,2048]{1,0:T(8,128)(2,1)} %shard_map.145) | data formatting | bytes 262144
where the time goes:
time: 104 us; the launch traced here: 102 us
  Pallas kernels  100 us (96%)
  local copies, waits for them, and re-layouts  1.57 us (2%)
    pallas_call x1, Pallas kernels, body(): pl.pallas_call(functools.partial(kernel, n, S), out_shape=jax.ShapeDtypeS...  100 us

commit v1 on v0

v1 whole, which is shorter than its diff:
```python
import functools

import jax
import jax.numpy as jnp
from jax import lax
from jax.experimental import pallas as pl
from jax.experimental.pallas import tpu as pltpu
from jax.sharding import PartitionSpec as P

HD = 256
EPS = 1e-06
STAT_ROWS = 8
LANES = 128
SOURCE_CHUNKS = 4
COLUMN_CHUNKS = 4
GROUP_ROWS = 256
MESH = pl.DeviceIdType.MESH
BF = jnp.bfloat16
F32 = jnp.float32


def normed_rows(wide, gain):
    return wide * lax.rsqrt(jnp.mean(wide * wide, axis=-1, keepdims=True) + EPS) * gain


def mm(a, b):
    return jnp.dot(a, b, preferred_element_type=F32)


def scope(name):
    return jax.named_scope(name)


def kernel(
    n,
    S,
    source,
    target,
    source_gain_in,
    attend_gain_in,
    query_weight,
    key_weight,
    value_weight,
    out_weight,
    mixer_gain_in,
    gate_weight,
    up_weight,
    gate_taps_in,
    up_taps_in,
    down_weight,
    final_gain_in,
    result,
    source_gain,
    attend_gain,
    mixer_gain,
    final_gain,
    gate_taps,
    up_taps,
    sv,
    traw,
    wq,
    wkv,
    wo,
    wg,
    wu,
    wd,
    xs,
    xt,
    kv,
    qall,
    osend,
    orecv,
    ssend,
    srecv,
    pf,
    att,
    p1s,
    p1r,
    p2s,
    p2r,
    dpf,
    d1s,
    d1r,
    d2s,
    d2r,
    hs,
    hr,
    gpad,
    upad,
    hid,
    residual,
    out_rows,
    load_sem,
    tr_send,
    tr_recv,
    n_send,
    n_recv,
    sx_send,
    sx_recv,
    sd_send,
    sd_recv,
    q_send,
    q_recv,
    r_send,
    r_recv,
    s_send,
    s_recv,
    p1_send,
    p1_recv,
    p2_send,
    p2_recv,
    d1_send,
    d1_recv,
    d2_send,
    d2_recv,
    h_send,
    h_recv,
):
    X = n // 2
    Rs, D = source.shape
    Rt = target.shape[0]
    W = wq.shape[2]
    H = 2 * Rt
    T = n * Rt
    heads = W // HD
    F = wg.shape[0]
    NC = xs.shape[1]
    RC = Rs // NC
    C = p1s.shape[2]
    DC = D // C
    scale = HD ** (-0.5)
    t = lax.axis_index("tp")
    s = lax.axis_index("sp")
    x = lax.div(t, 2)
    c = lax.rem(t, 2)
    other = 1 - c
    peer = x * 2 + other
    pending = []

    def chip_at(k):
        return lax.rem(x + k, X)

    def remote(src, dst, ss, rs, axis, where):
        return pltpu.make_async_remote_copy(
            src_ref=src,
            dst_ref=dst,
            send_sem=ss,
            recv_sem=rs,
            device_id={axis: where},
            device_id_type=MESH,
        )

    def launch(copy):
        copy.start()
        pending.append(copy)

    far_blocks = []
    low = s * 0
    high = low + (S - 1)
    for _ in range(S - 1):
        left = lax.div(2 * s - low - high + S, S)
        far_blocks.append(left * low + (1 - left) * high)
        low = low + left
        high = high - (1 - left)

    barrier = pltpu.get_barrier_semaphore()
    pl.semaphore_signal(barrier, inc=1, device_id={"tp": peer}, device_id_type=MESH)
    for k in range(1, X):
        pl.semaphore_signal(
            barrier, inc=1, device_id={"tp": chip_at(k) * 2 + c}, device_id_type=MESH
        )
    for block in far_blocks:
        pl.semaphore_signal(barrier, inc=1, device_id={"sp": block}, device_id_type=MESH)

    loads = iter(range(22))

    def load(src, dst):
        return pltpu.make_async_copy(src, dst, load_sem.at[next(loads)])

    load_t = load(target, traw.at[x])
    load_s = load(source, sv)
    load_small = [
        load(attend_gain_in, attend_gain),
        load(source_gain_in, source_gain),
    ]
    load_late = [
        load(mixer_gain_in, mixer_gain),
        load(final_gain_in, final_gain),
        load(gate_taps_in, gate_taps),
        load(up_taps_in, up_taps),
    ]
    load_q = [load(query_weight.at[l], wq.at[l]) for l in range(2)]
    load_kv = [
        [load(key_weight.at[l], wkv.at[2 * l]), load(value_weight.at[l], wkv.at[2 * l + 1])]
        for l in range(2)
    ]
    load_o = [load(out_weight.at[l], wo.at[l]) for l in range(2)]
    load_m = [load(gate_weight, wg), load(up_weight, wu), load(down_weight, wd)]
    for copy in [load_t, *load_small, load_s, load_q[0]]:
        copy.start()

    def target_copy(k, where):
        return remote(traw.at[k], traw.at[k], tr_send.at[where], tr_recv.at[k], "tp", where * 2 + c)

    def normed_copy(a, k, core):
        return remote(xt.at[a, k, core], xt.at[a, k, core], n_send.at[a, k], n_recv.at[a, k], "tp", peer)

    def source_copy(ch, k, where):
        return remote(
            xs.at[k, ch, c], xs.at[k, ch, c], sx_send.at[ch, where], sx_recv.at[ch, k], "tp", where * 2 + c
        )

    def source_peer(ch, k, core):
        return remote(
            xs.at[k, ch, core], xs.at[k, ch, core], sd_send.at[ch, k], sd_recv.at[ch, k], "tp", peer
        )

    def share_rows(a, k, gain):
        xt[a, k, c] = normed_rows(residual[k], gain).astype(BF)
        launch(normed_copy(a, k, c))

    def shared_rows(a, k):
        normed_copy(a, k, other).wait_recv()
        return xt[a, k].reshape(H, D)

    def query_copy(layer, k, j, block, where):
        return remote(
            qall.at[layer, k, block],
            qall.at[layer, k, block],
            q_send.at[layer, k, j],
            q_recv.at[layer, k, block],
            "sp",
            where,
        )

    def send_queries(layer, k):
        qall[layer, k, s] = mm(shared_rows(layer, k), wq[layer]).astype(BF)
        for j, block in enumerate(far_blocks):
            launch(query_copy(layer, k, j, s, block))

    def project_chip(layer):
        rows = xs[x].reshape(2 * Rs, D)

        def one(j, carry):
            kv[j, x] = mm(rows, wkv[j]).astype(BF).reshape(NC, 2 * RC, W)
            return carry

        lax.fori_loop(2 * layer, 2 * layer + 2, one, 0)

    def project_chunk(low, high, k, ch):
        rows = xs[k, ch].reshape(2 * RC, D)

        def one(j, carry):
            kv[j, k, ch] = mm(rows, wkv[j]).astype(BF)
            return carry

        lax.fori_loop(low, high, one, 0)

    def sums_copy(layer, k, j, slot, block):
        return remote(
            osend.at[layer, k, block],
            orecv.at[layer, k, slot],
            r_send.at[layer, k, j],
            r_recv.at[layer, k, slot],
            "sp",
            block,
        )

    def stats_copy(layer, k, j, slot, block):
        return remote(
            ssend.at[layer, k, block],
            srecv.at[layer, k, slot],
            s_send.at[layer, k, j],
            s_recv.at[layer, k, slot],
            "sp",
            block,
        )

    G = max(1, min(S, GROUP_ROWS // H))
    while S % G:
        G -= 1

    def attend(layer, k):
        for j, block in enumerate(far_blocks):
            query_copy(layer, k, j, block, block).wait_recv()

        def group(base):
            blocks = pl.ds(base, G)
            lanes = lax.broadcasted_iota(jnp.int32, (G * H, LANES), 1)
            packed = jnp.zeros((G * H, LANES), F32)
            for h in range(heads):
                cols = slice(h * HD, (h + 1) * HD)
                query = qall[layer, k, blocks, :, cols].reshape(G * H, HD)
                keys = kv[2 * layer, :, :, :, cols].reshape(n * Rs, HD)
                values = kv[2 * layer + 1, :, :, :, cols].reshape(n * Rs, HD)
                scores = (
                    lax.dot_general(
                        query, keys, (((1,), (1,)), ((), ())), preferred_element_type=F32
                    )
                    * scale
                )
                top = jnp.max(scores, axis=-1, keepdims=True)
                raised = jnp.exp(scores - top)
                total = jnp.sum(raised, axis=-1, keepdims=True)
                osend[layer, k, blocks, :, cols] = (
                    mm(raised.astype(BF), values).astype(BF).reshape(G, H, HD)
                )
                packed = jnp.where(lanes == 2 * h, top, packed)
                packed = jnp.where(lanes == 2 * h + 1, total, packed)
            stats = packed.T[:STAT_ROWS]
            for b in range(G):
                ssend[layer, k, base + b] = stats[:, b * H : (b + 1) * H]

        if G == S:
            group(0)
        else:

            def one(g, carry):
                group(g * G)
                return carry

            lax.fori_loop(0, S // G, one, 0)
        for j, block in enumerate(far_blocks):
            launch(stats_copy(layer, k, j, s, block))
            launch(sums_copy(layer, k, j, s, block))
        orecv[layer, k, s] = osend[layer, k, s]
        srecv[layer, k, s] = ssend[layer, k, s]

    def pair_copy(layer, k, ch):
        return remote(
            p1s.at[layer, k, ch],
            p1r.at[layer, k, ch],
            p1_send.at[layer, k, ch],
            p1_recv.at[layer, k, ch],
            "tp",
            peer,
        )

    def chip_copy(layer, k, ch, slot, where):
        return remote(
            p2s.at[layer, k, ch],
            p2r.at[layer, k, ch, slot],
            p2_send.at[layer, k, ch, where],
            p2_recv.at[layer, k, ch, slot],
            "tp",
            where * 2 + c,
        )

    def combine(layer, k):
        for j, block in enumerate(far_blocks):
            stats_copy(layer, k, j, block, block).wait_recv()
            sums_copy(layer, k, j, block, block).wait_recv()
        rows = srecv[layer, k].reshape(S * STAT_ROWS, H)
        if S * STAT_ROWS < LANES:
            rows = jnp.concatenate([rows, jnp.zeros((LANES - S * STAT_ROWS, H), F32)], axis=0)
        stats = rows.T
        for h in range(heads):
            cols = slice(h * HD, (h + 1) * HD)
            tops = [stats[:, b * STAT_ROWS + 2 * h :][:, :1] for b in range(S)]
            highest = functools.reduce(jnp.maximum, tops)
            total = jnp.zeros((H, 1), F32)
            summed = jnp.zeros((H, HD), F32)
            for b in range(S):
                factor = jnp.exp(tops[b] - highest)
                total = total + factor * stats[:, b * STAT_ROWS + 2 * h + 1 :][:, :1]
                summed = summed + factor * orecv[layer, k, b, :, cols].astype(F32)
            att[k, :, cols] = (summed / total).astype(BF)
        rows = att[k]
        for ch in range(C):
            cols = slice(ch * DC, (ch + 1) * DC)
            pf[k, :, :, cols] = mm(rows, wo[layer, :, cols]).reshape(2, Rt, DC)
            p1s[layer, k, ch] = pf[k, other, :, cols].astype(BF)
            launch(pair_copy(layer, k, ch))

    def spread(layer, k):
        for ch in range(C):
            cols = slice(ch * DC, (ch + 1) * DC)
            pair_copy(layer, k, ch).wait_recv()
            chip_sum = pf[k, c, :, cols] + p1r[layer, k, ch].astype(F32)
            p2s[layer, k, ch] = chip_sum.astype(BF)
            for i in range(1, X):
                launch(chip_copy(layer, k, ch, x, chip_at(i)))
            residual[k, :, cols] = residual[k, :, cols] + chip_sum

    def settle(layer, k, gain):
        for ch in range(C):
            cols = slice(ch * DC, (ch + 1) * DC)
            for i in range(1, X):
                chip_copy(layer, k, ch, chip_at(i), chip_at(i)).wait_recv()
                residual[k, :, cols] = residual[k, :, cols] + p2r[
                    layer, k, ch, chip_at(i)
                ].astype(F32)
        share_rows(layer + 1, k, gain)

    def finish_read(layer, gain, follow):
        for k in range(X):
            with scope(f"combine{layer}{k}"):
                combine(layer, k)
            if k:
                with scope(f"settle{layer}{k - 1}"):
                    settle(layer, k - 1, gain)
            with scope(f"spread{layer}{k}"):
                spread(layer, k)
            if k:
                with scope(f"follow{layer}{k - 1}"):
                    follow(k - 1)
        with scope(f"settle{layer}{X - 1}"):
            settle(layer, X - 1, gain)
        with scope(f"follow{layer}{X - 1}"):
            follow(X - 1)

    load_t.wait()
    with scope("barrier"):
        pl.semaphore_wait(barrier, X + S - 1)
    for i in range(1, X):
        launch(target_copy(x, chip_at(i)))
    for copy in load_kv[0]:
        copy.start()
    for copy in load_small:
        copy.wait()
    residual[x] = traw[x].astype(F32)
    share_rows(0, x, attend_gain[0:1])
    load_s.wait()
    with scope("norm_source"):
        for ch in range(NC):
            rows = sv[ch * RC : (ch + 1) * RC].astype(F32)
            xs[x, ch, c] = normed_rows(rows, source_gain[...]).astype(BF)
            for i in range(1, X):
                launch(source_copy(ch, x, chip_at(i)))
            launch(source_peer(ch, x, c))
    with scope("q0own"):
        load_q[0].wait()
        send_queries(0, x)
    for copy in load_kv[1]:
        copy.start()
    with scope("proj_chip0"):
        for ch in range(NC):
            source_peer(ch, x, other).wait_recv()
        for copy in load_kv[0]:
            copy.wait()
        project_chip(0)
    with scope("target_far"):
        for i in range(1, X):
            k = chip_at(i)
            target_copy(k, k).wait_recv()
            residual[k] = traw[k].astype(F32)
            share_rows(0, k, attend_gain[0:1])
    for copy in [load_q[1], *load_o]:
        copy.start()
    with scope("proj_chip1"):
        for copy in load_kv[1]:
            copy.wait()
        project_chip(1)
    with scope("q0far"):
        for i in range(1, X):
            send_queries(0, chip_at(i))
    for copy in [*load_late, *load_m]:
        copy.start()
    for ch in range(NC):
        with scope(f"forward{ch}"):
            for i in range(1, X):
                k = chip_at(i)
                source_copy(ch, k, k).wait_recv()
                launch(source_peer(ch, k, c))
        if ch:
            with scope(f"proj{ch - 1}"):
                for i in range(1, X):
                    source_peer(ch - 1, chip_at(i), other).wait_recv()
                    project_chunk(0, 4, chip_at(i), ch - 1)
    with scope("proj_last"):
        for i in range(1, X):
            source_peer(NC - 1, chip_at(i), other).wait_recv()
            project_chunk(0, 2, chip_at(i), NC - 1)
    for k in range(X):
        with scope(f"attend0{k}"):
            attend(0, k)
    with scope("proj_rest"):
        for i in range(1, X):
            project_chunk(2, 4, chip_at(i), NC - 1)
    for copy in [*load_o, load_q[1]]:
        copy.wait()
    finish_read(0, attend_gain[1:2], lambda k: send_queries(1, k))
    for k in range(X):
        with scope(f"attend1{k}"):
            attend(1, k)
    for copy in [*load_late, *load_m]:
        copy.wait()
    pads = ((gpad, wg), (upad, wu))

    def halo_out(number):
        return remote(
            hs.at[number],
            hr.at[number],
            h_send.at[number],
            h_recv.at[number],
            "sp",
            lax.rem(s + 1, S),
        )

    def lift(k):
        mixed = shared_rows(2, k)
        for number, (pad, weight) in enumerate(pads):
            lifted = (
                lax.dot_general(
                    mixed, weight[...], (((1,), (1,)), ((), ())), preferred_element_type=F32
                )
                .astype(BF)
                .astype(F32)
            )
            if k == X - 1:
                hs[number] = lifted[H - 8 :]

                @pl.when(s < S - 1)
                def _():
                    halo_out(number).start()

            pad[8 + k * H : 8 + (k + 1) * H] = lifted

    finish_read(1, mixer_gain[...], lift)

    def hidden_rows(start, stop):
        def convolved(pad, taps):
            return (
                taps[0:1] * pad[6 + start : 6 + stop]
                + taps[1:2] * pad[7 + start : 7 + stop]
                + taps[2:3] * pad[8 + start : 8 + stop]
            )

        gate = convolved(gpad, gate_taps)
        hid[start:stop] = (gate / (1.0 + jnp.exp(-gate)) * convolved(upad, up_taps)).astype(BF)

    with scope("hidden"):
        hidden_rows(16, T)

    @pl.when(s == 0)
    def _():
        for pad, _weight in pads:
            pad[:8] = jnp.zeros((8, F), F32)

    @pl.when(s > 0)
    def _():
        for number, (pad, _weight) in enumerate(pads):
            halo_out(number).wait_recv()
            pad[:8] = hr[number]

    @pl.when(s < S - 1)
    def _():
        for number in range(2):
            halo_out(number).wait_send()

    hidden_rows(0, 16)

    def down_pair(ch):
        return remote(d1s.at[ch], d1r.at[ch], d1_send.at[ch], d1_recv.at[ch], "tp", peer)

    def down_chip(ch, i, slot, where):
        return remote(
            d2s.at[ch, i],
            d2r.at[ch, slot],
            d2_send.at[ch, i],
            d2_recv.at[ch, slot],
            "tp",
            where * 2 + c,
        )

    with scope("down_mm"):
        rows = hid[...]
        for ch in range(C):
            cols = slice(ch * DC, (ch + 1) * DC)
            dpf[:, :, :, cols] = mm(rows, wd[:, cols]).reshape(X, 2, Rt, DC)
            d1s[ch] = dpf[:, other, :, cols].astype(BF)
            launch(down_pair(ch))
    with scope("down_pair"):
        for ch in range(C):
            cols = slice(ch * DC, (ch + 1) * DC)
            down_pair(ch).wait_recv()
            for i in range(1, X):
                k = chip_at(i)
                d2s[ch, i] = (dpf[k, c, :, cols] + d1r[ch, k].astype(F32)).astype(BF)
                launch(down_chip(ch, i, x, k))
            residual[x, :, cols] = (
                residual[x, :, cols] + dpf[x, c, :, cols] + d1r[ch, x].astype(F32)
            )
    with scope("down_far"):
        for ch in range(C):
            cols = slice(ch * DC, (ch + 1) * DC)
            for i in range(1, X):
                k = chip_at(i)
                down_chip(ch, i, k, k).wait_recv()
                residual[x, :, cols] = residual[x, :, cols] + d2r[ch, k].astype(F32)
    out_rows[...] = normed_rows(residual[x], final_gain[...]).astype(BF)
    write = load(out_rows, result)
    write.start()
    for copy in pending:
        copy.wait_send()
    write.wait()


def body(n, S, *arrays):
    (
        source,
        target,
        source_gain,
        attend_gain,
        query_weight,
        key_weight,
        value_weight,
        out_weight,
        mixer_gain,
        gate_weight,
        up_weight,
        gate_taps,
        up_taps,
        down_weight,
        final_gain,
    ) = arrays
    Rs, D = source.shape
    Rt = target.shape[0]
    W = query_weight.shape[2]
    F = gate_weight.shape[1]
    T = n * Rt
    H = 2 * Rt
    X = n // 2
    NC = SOURCE_CHUNKS
    C = COLUMN_CHUNKS
    RC = Rs // NC
    DC = D // C
    hbm = pl.BlockSpec(memory_space=pl.ANY)
    dma = pltpu.SemaphoreType.DMA
    scratch = [
        pltpu.VMEM((1, D), F32),
        pltpu.VMEM((2, D), F32),
        pltpu.VMEM((1, D), F32),
        pltpu.VMEM((1, D), F32),
        pltpu.VMEM((3, F), F32),
        pltpu.VMEM((3, F), F32),
        pltpu.VMEM((Rs, D), BF),
        pltpu.VMEM((X, Rt, D), BF),
        pltpu.VMEM((2, D, W), BF),
        pltpu.VMEM((4, D, W), BF),
        pltpu.VMEM((2, W, D), BF),
        pltpu.VMEM((F, D), BF),
        pltpu.VMEM((F, D), BF),
        pltpu.VMEM((F, D), BF),
        pltpu.VMEM((X, NC, 2, RC, D), BF),
        pltpu.VMEM((3, X, 2, Rt, D), BF),
        pltpu.VMEM((4, X, NC, 2 * RC, W), BF),
        pltpu.VMEM((2, X, S, H, W), BF),
        pltpu.VMEM((2, X, S, H, W), BF),
        pltpu.VMEM((2, X, S, H, W), BF),
        pltpu.VMEM((2, X, S, STAT_ROWS, H), F32),
        pltpu.VMEM((2, X, S, STAT_ROWS, H), F32),
        pltpu.VMEM((X, 2, Rt, D), F32),
        pltpu.VMEM((X, H, W), BF),
        pltpu.VMEM((2, X, C, Rt, DC), BF),
        pltpu.VMEM((2, X, C, Rt, DC), BF),
        pltpu.VMEM((2, X, C, Rt, DC), BF),
        pltpu.VMEM((2, X, C, X, Rt, DC), BF),
        pltpu.VMEM((X, 2, Rt, D), F32),
        pltpu.VMEM((C, X, Rt, DC), BF),
        pltpu.VMEM((C, X, Rt, DC), BF),
        pltpu.VMEM((C, X, Rt, DC), BF),
        pltpu.VMEM((C, X, Rt, DC), BF),
        pltpu.VMEM((2, 8, F), F32),
        pltpu.VMEM((2, 8, F), F32),
        pltpu.VMEM((T + 8, F), F32),
        pltpu.VMEM((T + 8, F), F32),
        pltpu.VMEM((T, F), BF),
        pltpu.VMEM((X, Rt, D), F32),
        pltpu.VMEM((Rt, D), BF),
        dma((22,)),
        dma((X,)),
        dma((X,)),
        dma((3, X)),
        dma((3, X)),
        dma((NC, X)),
        dma((NC, X)),
        dma((NC, X)),
        dma((NC, X)),
        dma((2, X, S)),
        dma((2, X, S)),
        dma((2, X, S)),
        dma((2, X, S)),
        dma((2, X, S)),
        dma((2, X, S)),
        dma((2, X, C)),
        dma((2, X, C)),
        dma((2, X, C, X)),
        dma((2, X, C, X)),
        dma((C,)),
        dma((C,)),
        dma((C, X)),
        dma((C, X)),
        dma((2,)),
        dma((2,)),
    ]
    return pl.pallas_call(
        functools.partial(kernel, n, S),
        out_shape=jax.ShapeDtypeStruct((Rt, D), BF),
        in_specs=[hbm] * 15,
        out_specs=hbm,
        scratch_shapes=scratch,
        compiler_params=pltpu.CompilerParams(
            collective_id=0, has_side_effects=True, vmem_limit_bytes=67043328
        ),
    )(
        source,
        target,
        source_gain.reshape(1, D),
        attend_gain,
        query_weight,
        key_weight,
        value_weight,
        out_weight,
        mixer_gain.reshape(1, D),
        gate_weight.T,
        up_weight.T,
        gate_taps,
        up_taps,
        down_weight,
        final_gain.reshape(1, D),
    )


def solution(mesh):
    placed = (
        P(("grp", "sp", "tp"), None),
        P(("grp", "sp", "tp"), None),
        P(),
        P(),
        P(None, None, "tp"),
        P(None, None, "tp"),
        P(None, None, "tp"),
        P(None, "tp", None),
        P(),
        P(None, "tp"),
        P(None, "tp"),
        P(None, "tp"),
        P(None, "tp"),
        P("tp", None),
        P(),
    )
    return jax.shard_map(
        functools.partial(body, mesh.shape["tp"], mesh.shape["sp"]),
        mesh=mesh,
        in_specs=placed,
        out_specs=P(("grp", "sp", "tp"), None),
        check_vma=False,
    )
```

time: 104 us -> 89.8 us (0.86); the launches traced: 102 us -> 89.7 us
  Pallas kernels: 100 us -> 88.1 us
    pallas_call x1, Pallas kernels: 100 us -> 88.1 us  [body(): pl.pallas_call(functools.partial(kernel, n, S), out_shape=jax.ShapeDtypeS...]
where the time goes in v1:
time: 89.8 us; the launch traced here: 89.7 us
  Pallas kernels  88.1 us (98%)
  local copies, waits for them, and re-layouts  1.57 us (2%)
    pallas_call x1, Pallas kernels, body(): pl.pallas_call(functools.partial(kernel, n, S), out_shape=jax.ShapeDtypeS...  88.1 us

profile of v1, /device:TPU:0, one launch (start us, length us, event | category | flops | bytes accessed | tf_op | source)
XLA Modules:
  0.0 89.7 jit_solution(1273880870163634661)
XLA Ops:
  0.0 88.1 %shard_map.145 = bf16[32,2048]{1,0:T(8,128)(2,1)} custom-call(bf16[128,2048]{1,0:T(8,128)(2,1)} %source.1, bf16[32,2048]{1,0:T(8,128)(2,1)} %target.1, f32[1,2048]{1,0:T(1,128)} %bitcast.7, f32[2,2048]{1,0:T(2,128)} %attend_gain_in.1, bf16[2,2048,512]{2,1,0:T(8,128)(2,1)} %query_weight.1, bf16[2,2048,512]{2,1,0:T(8,128)(2,1)} %key_weight.1, ...), custom_call_target="tpu_custom_call" | custom-call | tf_op jit(solution)/shard_map/pallas_call | solution.py:697
  88.1 1.6 %copy.17 = bf16[32,2048]{1,0:T(8,128)(2,1)} copy(bf16[32,2048]{1,0:T(8,128)(2,1)} %shard_map.145) | data formatting | bytes 262144

commit v2 on v1

--- a/solution.py
+++ b/solution.py
@@ -63,6 +63,8 @@
     wo,
     wg,
     wu,
+    wgt,
+    wut,
     wd,
     xs,
     xt,
@@ -89,7 +91,6 @@
     upad,
     hid,
     residual,
-    out_rows,
     load_sem,
     tr_send,
     tr_recv,
@@ -136,6 +137,7 @@
     other = 1 - c
     peer = x * 2 + other
     pending = []
+    order = [*reversed(range(X))]
 
     def chip_at(k):
         return lax.rem(x + k, X)
@@ -149,6 +151,10 @@
             device_id={axis: where},
             device_id_type=MESH,
         )
+
+    def drain():
+        while pending:
+            pending.pop().wait_send()
 
     def launch(copy):
         copy.start()
@@ -238,23 +244,23 @@
         for j, block in enumerate(far_blocks):
             launch(query_copy(layer, k, j, s, block))
 
-    def project_chip(layer):
-        rows = xs[x].reshape(2 * Rs, D)
+    def project_chip(layer, k):
+        rows = xs[k].reshape(2 * Rs, D)
 
         def one(j, carry):
-            kv[j, x] = mm(rows, wkv[j]).astype(BF).reshape(NC, 2 * RC, W)
+            kv[j, k] = mm(rows, wkv[j]).astype(BF).reshape(NC, 2 * RC, W)
             return carry
 
         lax.fori_loop(2 * layer, 2 * layer + 2, one, 0)
 
-    def project_chunk(low, high, k, ch):
+    def project_chunk(k, ch):
         rows = xs[k, ch].reshape(2 * RC, D)
 
         def one(j, carry):
             kv[j, k, ch] = mm(rows, wkv[j]).astype(BF)
             return carry
 
-        lax.fori_loop(low, high, one, 0)
+        lax.fori_loop(0, 2, one, 0)
 
     def sums_copy(layer, k, j, slot, block):
         return remote(
@@ -393,25 +399,32 @@
         share_rows(layer + 1, k, gain)
 
     def finish_read(layer, gain, follow):
-        for k in range(X):
+        def close(k):
+            with scope(f"settle{layer}{k}"):
+                settle(layer, k, gain)
+            with scope(f"follow{layer}{k}"):
+                follow(k)
+
+        for i, k in enumerate(order):
             with scope(f"combine{layer}{k}"):
                 combine(layer, k)
-            if k:
-                with scope(f"settle{layer}{k - 1}"):
-                    settle(layer, k - 1, gain)
             with scope(f"spread{layer}{k}"):
                 spread(layer, k)
-            if k:
-                with scope(f"follow{layer}{k - 1}"):
-                    follow(k - 1)
-        with scope(f"settle{layer}{X - 1}"):
-            settle(layer, X - 1, gain)
-        with scope(f"follow{layer}{X - 1}"):
-            follow(X - 1)
-
-    load_t.wait()
+            if i:
+                close(order[i - 1])
+        close(order[-1])
+
+    def turn_weight(src, dst):
+        def one(j, carry):
+            rows = pl.ds(pl.multiple_of(j * GROUP_ROWS, GROUP_ROWS), GROUP_ROWS)
+            dst[rows] = src[:, rows].T
+            return carry
+
+        lax.fori_loop(0, D // GROUP_ROWS, one, 0)
+
     with scope("barrier"):
         pl.semaphore_wait(barrier, X + S - 1)
+    load_t.wait()
     for i in range(1, X):
         launch(target_copy(x, chip_at(i)))
     for copy in load_kv[0]:
@@ -438,7 +451,7 @@
             source_peer(ch, x, other).wait_recv()
         for copy in load_kv[0]:
             copy.wait()
-        project_chip(0)
+        project_chip(0, x)
     with scope("target_far"):
         for i in range(1, X):
             k = chip_at(i)
@@ -450,7 +463,7 @@
     with scope("proj_chip1"):
         for copy in load_kv[1]:
             copy.wait()
-        project_chip(1)
+        project_chip(1, x)
     with scope("q0far"):
         for i in range(1, X):
             send_queries(0, chip_at(i))
@@ -462,30 +475,30 @@
                 k = chip_at(i)
                 source_copy(ch, k, k).wait_recv()
                 launch(source_peer(ch, k, c))
-        if ch:
-            with scope(f"proj{ch - 1}"):
-                for i in range(1, X):
-                    source_peer(ch - 1, chip_at(i), other).wait_recv()
-                    project_chunk(0, 4, chip_at(i), ch - 1)
-    with scope("proj_last"):
-        for i in range(1, X):
-            source_peer(NC - 1, chip_at(i), other).wait_recv()
-            project_chunk(0, 2, chip_at(i), NC - 1)
-    for k in range(X):
+        with scope(f"proj{ch}"):
+            for i in range(1, X):
+                source_peer(ch, chip_at(i), other).wait_recv()
+                project_chunk(chip_at(i), ch)
+    for k in order:
         with scope(f"attend0{k}"):
             attend(0, k)
     with scope("proj_rest"):
         for i in range(1, X):
-            project_chunk(2, 4, chip_at(i), NC - 1)
+            project_chip(1, chip_at(i))
+    drain()
     for copy in [*load_o, load_q[1]]:
         copy.wait()
     finish_read(0, attend_gain[1:2], lambda k: send_queries(1, k))
-    for k in range(X):
+    for copy in [*load_late, *load_m]:
+        copy.wait()
+    turns = [(wg, wgt), (wu, wut)]
+    for i, k in enumerate(order):
+        with scope(f"turn{i}"):
+            for turn in turns[i * 2 // X : (i + 1) * 2 // X]:
+                turn_weight(*turn)
         with scope(f"attend1{k}"):
             attend(1, k)
-    for copy in [*load_late, *load_m]:
-        copy.wait()
-    pads = ((gpad, wg), (upad, wu))
+    pads = ((gpad, wgt), (upad, wut))
 
     def halo_out(number):
         return remote(
@@ -500,13 +513,7 @@
     def lift(k):
         mixed = shared_rows(2, k)
         for number, (pad, weight) in enumerate(pads):
-            lifted = (
-                lax.dot_general(
-                    mixed, weight[...], (((1,), (1,)), ((), ())), preferred_element_type=F32
-                )
-                .astype(BF)
-                .astype(F32)
-            )
+            lifted = mm(mixed, weight[...]).astype(BF).astype(F32)
             if k == X - 1:
                 hs[number] = lifted[H - 8 :]
 
@@ -581,6 +588,9 @@
             residual[x, :, cols] = (
                 residual[x, :, cols] + dpf[x, c, :, cols] + d1r[ch, x].astype(F32)
             )
+    with scope("drain"):
+        last = [pending.pop() for _ in range(C * (X - 1))]
+        drain()
     with scope("down_far"):
         for ch in range(C):
             cols = slice(ch * DC, (ch + 1) * DC)
@@ -588,12 +598,9 @@
                 k = chip_at(i)
                 down_chip(ch, i, k, k).wait_recv()
                 residual[x, :, cols] = residual[x, :, cols] + d2r[ch, k].astype(F32)
-    out_rows[...] = normed_rows(residual[x], final_gain[...]).astype(BF)
-    write = load(out_rows, result)
-    write.start()
-    for copy in pending:
+    result[...] = normed_rows(residual[x], final_gain[...]).astype(BF)
+    for copy in last:
         copy.wait_send()
-    write.wait()
 
 
 def body(n, S, *arrays):
@@ -641,6 +648,8 @@
         pltpu.VMEM((2, W, D), BF),
         pltpu.VMEM((F, D), BF),
         pltpu.VMEM((F, D), BF),
+        pltpu.VMEM((D, F), BF),
+        pltpu.VMEM((D, F), BF),
         pltpu.VMEM((F, D), BF),
         pltpu.VMEM((X, NC, 2, RC, D), BF),
         pltpu.VMEM((3, X, 2, Rt, D), BF),
@@ -667,7 +676,6 @@
         pltpu.VMEM((T + 8, F), F32),
         pltpu.VMEM((T, F), BF),
         pltpu.VMEM((X, Rt, D), F32),
-        pltpu.VMEM((Rt, D), BF),
         dma((22,)),
         dma((X,)),
         dma((X,)),
@@ -696,12 +704,12 @@
     ]
     return pl.pallas_call(
         functools.partial(kernel, n, S),
-        out_shape=jax.ShapeDtypeStruct((Rt, D), BF),
+        out_shape=pltpu.VMEM((Rt, D), BF),
         in_specs=[hbm] * 15,
-        out_specs=hbm,
+        out_specs=pl.BlockSpec(memory_space=pltpu.VMEM),
         scratch_shapes=scratch,
         compiler_params=pltpu.CompilerParams(
-            collective_id=0, has_side_effects=True, vmem_limit_bytes=67043328
+            collective_id=0, has_side_effects=True, vmem_limit_bytes=66000000
         ),
     )(
         source,

time: 89.8 us -> 84.2 us (0.938)
  Pallas kernels: 88.1 us -> 83.4 us
  local copies, waits for them, and re-layouts: 1.57 us -> 0.66 us
    pallas_call x1, Pallas kernels: 88.1 us -> 83.4 us  [body(): pl.pallas_call(functools.partial(kernel, n, S), out_shape=pltpu.VMEM((Rt,...]
    unnamed x1, local copies, waits for them, and re-layouts: 1.57 us -> 0.66 us
where the time goes in v2:
time: 84.2 us; the launch traced here: 84.1 us
  Pallas kernels  83.4 us (99%)
    pallas_call x1, Pallas kernels, body(): pl.pallas_call(functools.partial(kernel, n, S), out_shape=pltpu.VMEM((Rt,...  83.4 us

profile of v2, /device:TPU:0, one launch (start us, length us, event | category | flops | bytes accessed | tf_op | source)
XLA Modules:
  0.0 84.1 jit_solution(4539859322031943093)
XLA Ops:
  0.0 83.4 %shard_map.145 = bf16[32,2048]{1,0:T(8,128)(2,1)S(1)} custom-call(bf16[128,2048]{1,0:T(8,128)(2,1)} %source.1, bf16[32,2048]{1,0:T(8,128)(2,1)} %target.1, f32[1,2048]{1,0:T(1,128)} %bitcast.7, f32[2,2048]{1,0:T(2,128)} %attend_gain_in.1, bf16[2,2048,512]{2,1,0:T(8,128)(2,1)} %query_weight.1, bf16[2,2048,512]{2,1,0:T(8,128)(2,1)} %key_weight.1, ...), custom_call_target="tpu_custom_call" | custom-call | tf_op jit(solution)/shard_map/pallas_call | solution.py:705
  83.4 0.7 copy.17

commit v3 on v2

v3 whole, which is shorter than its diff:
```python
import functools

import jax
import jax.numpy as jnp
from jax import lax
from jax.experimental import pallas as pl
from jax.experimental.pallas import tpu as pltpu
from jax.sharding import PartitionSpec as P

HD = 256
EPS = 1e-06
STAT_ROWS = 8
LANES = 128
SOURCE_CHUNKS = 4
STREAMS_PER_CHIP = 2
OUT_CHUNKS = 2
DOWN_CHUNKS = 4
GROUP_ROWS = 256
MESH = pl.DeviceIdType.MESH
BF = jnp.bfloat16
F32 = jnp.float32


def normed_rows(wide, gain):
    return wide * lax.rsqrt(jnp.mean(wide * wide, axis=-1, keepdims=True) + EPS) * gain


def mm(a, b):
    return jnp.dot(a, b, preferred_element_type=F32)


def scope(name):
    return jax.named_scope(name)


def kernel(
    n,
    S,
    source,
    target,
    source_gain_in,
    attend_gain_in,
    query_weight,
    key_weight,
    value_weight,
    out_weight,
    mixer_gain_in,
    gate_weight,
    up_weight,
    gate_taps_in,
    up_taps_in,
    down_weight,
    final_gain_in,
    result,
    source_gain,
    attend_gain,
    mixer_gain,
    final_gain,
    gate_taps,
    up_taps,
    sv,
    traw,
    wq,
    wkv,
    wo,
    wg,
    wu,
    wgt,
    wut,
    wd,
    xs,
    xt,
    kv,
    qall,
    osend,
    orecv,
    ssend,
    srecv,
    pf,
    att,
    p1s,
    p1r,
    p2s,
    p2r,
    dpf,
    d1s,
    d1r,
    d2s,
    d2r,
    hs,
    hr,
    gpad,
    upad,
    hid,
    residual,
    load_sem,
    sent,
    tr_recv,
    n_recv,
    sx_recv,
    sd_recv,
    own_recv,
    q_recv,
    cross_recv,
    r_recv,
    s_recv,
    p1_recv,
    p2_recv,
    d1_recv,
    d2_recv,
    h_recv,
):
    X = n // 2
    Rs, D = source.shape
    Rt = target.shape[0]
    W = wq.shape[2]
    T = n * Rt
    NS, Rh = residual.shape[:2]
    SUB = NS // X
    H = 2 * Rh
    heads = W // HD
    F = wg.shape[0]
    NC = xs.shape[1]
    RC = Rs // NC
    C = p1s.shape[2]
    C2 = d1s.shape[0]
    scale = HD ** (-0.5)
    t = lax.axis_index("tp")
    s = lax.axis_index("sp")
    x = lax.div(t, 2)
    c = lax.rem(t, 2)
    other = 1 - c
    peer = x * 2 + other
    offsets = range(1, X)
    order = [k * SUB + h for k in reversed(range(X)) for h in range(SUB)]

    def to_chip(i):
        return lax.rem(x + i, X)

    def from_chip(i):
        return lax.rem(x + X - i, X)

    def streams(k):
        return pl.ds(k * SUB, SUB)

    def remote(src, dst, ss, rs, axis, where):
        return pltpu.make_async_remote_copy(
            src_ref=src,
            dst_ref=dst,
            send_sem=ss,
            recv_sem=rs,
            device_id={axis: where},
            device_id_type=MESH,
        )

    def wait_for(sem, ref):
        remote(ref, ref, sent.at[0], sem, "tp", peer).wait_recv()

    def wait_sent(number, ref):
        remote(ref, ref, sent.at[number], own_recv.at[0], "tp", peer).wait_send()

    far_blocks = []
    low = s * 0
    high = low + (S - 1)
    for _ in range(S - 1):
        left = lax.div(2 * s - low - high + S, S)
        far_blocks.append(left * low + (1 - left) * high)
        low = low + left
        high = high - (1 - left)
    most = pl.ds(0, S - 1)
    half = S // 2
    RELAY = S % 2 == 0 and S > 2

    barrier = pltpu.get_barrier_semaphore()
    pl.semaphore_signal(barrier, inc=1, device_id={"tp": peer}, device_id_type=MESH)
    for i in offsets:
        pl.semaphore_signal(
            barrier, inc=1, device_id={"tp": to_chip(i) * 2 + c}, device_id_type=MESH
        )
    for block in far_blocks:
        pl.semaphore_signal(barrier, inc=1, device_id={"sp": block}, device_id_type=MESH)

    def load(number, src, dst):
        return pltpu.make_async_copy(src, dst, load_sem.at[number])

    load_t = load(0, target, traw.at[x])
    load_s = load(1, source, sv)
    load_small = [load(2, attend_gain_in, attend_gain), load(3, source_gain_in, source_gain)]
    load_late = [
        load(0, mixer_gain_in, mixer_gain),
        load(1, final_gain_in, final_gain),
        load(2, gate_taps_in, gate_taps),
        load(3, up_taps_in, up_taps),
    ]
    load_q = [load(4, query_weight.at[l], wq.at[l]) for l in range(2)]
    load_kv = [
        [
            load(5 + 2 * l, key_weight.at[l], wkv.at[2 * l]),
            load(6 + 2 * l, value_weight.at[l], wkv.at[2 * l + 1]),
        ]
        for l in range(2)
    ]
    load_o = [load(5 + l, out_weight.at[l], wo.at[l]) for l in range(2)]
    load_m = [load(9, gate_weight, wg), load(10, up_weight, wu), load(11, down_weight, wd)]
    for copy in [load_t, *load_small, load_s, load_q[0]]:
        copy.start()

    def share_rows(a, rows, number):
        remote(
            xt.at[a, rows, c], xt.at[a, rows, c], sent.at[1], n_recv.at[a, number], "tp", peer
        ).start()

    def await_rows(a, rows, number):
        wait_for(n_recv.at[a, number], xt.at[a, rows, other])

    def first_rows(k):
        rows = traw[k].astype(F32)
        residual[streams(k)] = rows.reshape(SUB, Rh, D)
        xt[0, streams(k), c] = normed_rows(rows, attend_gain[0:1]).astype(BF).reshape(SUB, Rh, D)
        share_rows(0, streams(k), k)

    def first_queries(k):
        await_rows(0, streams(k), k)
        rows = xt[0, streams(k)].reshape(SUB * H, D)
        qall[0, streams(k), s] = mm(rows, wq[0]).astype(BF).reshape(SUB, H, W)
        for block in far_blocks:
            mine = qall.at[0, streams(k), s]
            remote(mine, mine, sent.at[4], q_recv.at[0, k], "sp", block).start()

    def next_queries(j):
        await_rows(1, j, j)
        qall[1, j, s] = mm(xt[1, j].reshape(H, D), wq[1]).astype(BF)
        if RELAY:
            mine = qall.at[1, j, s]
            remote(mine, mine, sent.at[4], cross_recv.at[j], "sp", lax.rem(s + half, S)).start()
            to_mates(j, s)
        else:
            for block in far_blocks:
                mine = qall.at[1, j, s]
                remote(mine, mine, sent.at[4], q_recv.at[1, j], "sp", block).start()

    def to_mates(j, block):
        for m in range(1, half):
            mate = lax.div(s, half) * half + lax.rem(s + m, half)
            rows = qall.at[1, j, block]
            remote(rows, rows, sent.at[4], q_recv.at[1, j], "sp", mate).start()

    def relay(j):
        if RELAY:
            block = lax.rem(s + half, S)
            wait_for(cross_recv.at[j], qall.at[1, j, block])
            to_mates(j, block)

    def await_queries(j):
        count = 2 * (half - 1) if RELAY else S - 1
        wait_for(q_recv.at[1, j], qall.at[1, j, pl.ds(0, count)])

    def project_chip(layer, k):
        rows = xs[k].reshape(2 * Rs, D)

        def one(j, carry):
            kv[j, k] = mm(rows, wkv[j]).astype(BF).reshape(NC, 2 * RC, W)
            return carry

        lax.fori_loop(2 * layer, 2 * layer + 2, one, 0)

    def project_chunk(k, ch):
        rows = xs[k, ch].reshape(2 * RC, D)

        def one(j, carry):
            kv[j, k, ch] = mm(rows, wkv[j]).astype(BF)
            return carry

        lax.fori_loop(0, 2, one, 0)

    G = max(1, min(S, GROUP_ROWS // H))
    while S % G:
        G -= 1

    def attend(layer, j):
        def group(base):
            blocks = pl.ds(base, G)
            lanes = lax.broadcasted_iota(jnp.int32, (G * H, LANES), 1)
            packed = jnp.zeros((G * H, LANES), F32)
            for h in range(heads):
                cols = slice(h * HD, (h + 1) * HD)
                query = qall[layer, j, blocks, :, cols].reshape(G * H, HD)
                keys = kv[2 * layer, :, :, :, cols].reshape(n * Rs, HD)
                values = kv[2 * layer + 1, :, :, :, cols].reshape(n * Rs, HD)
                scores = (
                    lax.dot_general(
                        query, keys, (((1,), (1,)), ((), ())), preferred_element_type=F32
                    )
                    * scale
                )
                top = jnp.max(scores, axis=-1, keepdims=True)
                raised = jnp.exp(scores - top)
                total = jnp.sum(raised, axis=-1, keepdims=True)
                osend[layer, j, blocks, :, cols] = (
                    mm(raised.astype(BF), values).astype(BF).reshape(G, H, HD)
                )
                packed = jnp.where(lanes == 2 * h, top, packed)
                packed = jnp.where(lanes == 2 * h + 1, total, packed)
            stats = packed.T[:STAT_ROWS]
            for b in range(G):
                ssend[layer, j, base + b] = stats[:, b * H : (b + 1) * H]

        if G == S:
            group(0)
        else:

            def one(g, carry):
                group(g * G)
                return carry

            lax.fori_loop(0, S // G, one, 0)
        for block in far_blocks:
            for src, dst, number, sem in (
                (ssend, srecv, 6, s_recv),
                (osend, orecv, 5, r_recv),
            ):
                remote(
                    src.at[layer, j, block],
                    dst.at[layer, j, s],
                    sent.at[number],
                    sem.at[layer, j],
                    "sp",
                    block,
                ).start()
        orecv[layer, j, s] = osend[layer, j, s]
        srecv[layer, j, s] = ssend[layer, j, s]

    def combine(layer, j):
        wait_for(s_recv.at[layer, j], srecv.at[layer, j, most])
        wait_for(r_recv.at[layer, j], orecv.at[layer, j, most])
        rows = srecv[layer, j].reshape(S * STAT_ROWS, H)
        if S * STAT_ROWS < LANES:
            rows = jnp.concatenate([rows, jnp.zeros((LANES - S * STAT_ROWS, H), F32)], axis=0)
        stats = rows.T
        for h in range(heads):
            cols = slice(h * HD, (h + 1) * HD)
            tops = [stats[:, b * STAT_ROWS + 2 * h :][:, :1] for b in range(S)]
            highest = functools.reduce(jnp.maximum, tops)
            total = jnp.zeros((H, 1), F32)
            summed = jnp.zeros((H, HD), F32)
            for b in range(S):
                factor = jnp.exp(tops[b] - highest)
                total = total + factor * stats[:, b * STAT_ROWS + 2 * h + 1 :][:, :1]
                summed = summed + factor * orecv[layer, j, b, :, cols].astype(F32)
            att[j, :, cols] = (summed / total).astype(BF)
        rows = att[j]
        for ch in range(C):
            cols = slice(ch * (D // C), (ch + 1) * (D // C))
            pf[j, :, :, cols] = mm(rows, wo[layer, :, cols]).reshape(2, Rh, D // C)
            p1s[layer, j, ch] = pf[j, other, :, cols].astype(BF)
            remote(
                p1s.at[layer, j, ch],
                p1r.at[layer, j, ch],
                sent.at[7],
                p1_recv.at[layer, j, ch],
                "tp",
                peer,
            ).start()

    def spread(layer, j):
        for ch in range(C):
            cols = slice(ch * (D // C), (ch + 1) * (D // C))
            wait_for(p1_recv.at[layer, j, ch], p1r.at[layer, j, ch])
            chip_sum = pf[j, c, :, cols] + p1r[layer, j, ch].astype(F32)
            p2s[layer, j, ch] = chip_sum.astype(BF)
            for i in offsets:
                remote(
                    p2s.at[layer, j, ch],
                    p2r.at[layer, j, ch, i - 1],
                    sent.at[8],
                    p2_recv.at[layer, j, ch, i - 1],
                    "tp",
                    to_chip(i) * 2 + c,
                ).start()
            residual[j, :, cols] = residual[j, :, cols] + chip_sum

    def settle(layer, j, gain):
        for ch in range(C):
            cols = slice(ch * (D // C), (ch + 1) * (D // C))
            for i in offsets:
                wait_for(p2_recv.at[layer, j, ch, i - 1], p2r.at[layer, j, ch, i - 1])
                residual[j, :, cols] = residual[j, :, cols] + p2r[layer, j, ch, i - 1].astype(F32)
        xt[layer + 1, j, c] = normed_rows(residual[j], gain).astype(BF)
        share_rows(layer + 1, j, j)

    def turn_weight(src, dst):
        def one(j, carry):
            rows = pl.ds(pl.multiple_of(j * GROUP_ROWS, GROUP_ROWS), GROUP_ROWS)
            dst[rows] = src[:, rows].T
            return carry

        lax.fori_loop(0, D // GROUP_ROWS, one, 0)

    with scope("barrier"):
        pl.semaphore_wait(barrier, X + S - 1)
    load_t.wait()
    for i in offsets:
        remote(
            traw.at[x], traw.at[x], sent.at[0], tr_recv.at[i - 1], "tp", to_chip(i) * 2 + c
        ).start()
    for copy in load_kv[0]:
        copy.start()
    for copy in load_small:
        copy.wait()
    first_rows(x)
    load_s.wait()
    with scope("norm_source"):
        for ch in range(NC):
            rows = sv[ch * RC : (ch + 1) * RC].astype(F32)
            xs[x, ch, c] = normed_rows(rows, source_gain[...]).astype(BF)
            mine = xs.at[x, ch, c]
            for i in offsets:
                remote(
                    mine, mine, sent.at[2], sx_recv.at[ch, i - 1], "tp", to_chip(i) * 2 + c
                ).start()
            remote(mine, mine, sent.at[3], own_recv.at[0], "tp", peer).start()
    with scope("q0own"):
        load_q[0].wait()
        first_queries(x)
    for copy in [*load_kv[1], *load_m, *load_late]:
        copy.start()
    with scope("proj_chip0"):
        wait_for(own_recv.at[0], xs.at[x, :, other])
        for copy in load_kv[0]:
            copy.wait()
        project_chip(0, x)
    with scope("target_far"):
        for i in offsets:
            k = from_chip(i)
            wait_for(tr_recv.at[i - 1], traw.at[k])
            first_rows(k)
    for copy in [load_q[1], *load_o]:
        copy.start()
    with scope("proj_chip1"):
        for copy in load_kv[1]:
            copy.wait()
        project_chip(1, x)
    with scope("q0far"):
        for i in offsets:
            first_queries(from_chip(i))
    turns = [(load_m[0], wg, wgt), (load_m[1], wu, wut)]
    for ch in range(NC):
        if ch and turns:
            with scope("turn"):
                copy, src, dst = turns.pop(0)
                copy.wait()
                turn_weight(src, dst)
        with scope(f"forward{ch}"):
            for i in offsets:
                landed = xs.at[from_chip(i), ch, c]
                wait_for(sx_recv.at[ch, i - 1], landed)
                remote(landed, landed, sent.at[3], sd_recv.at[ch, i - 1], "tp", peer).start()
        with scope(f"proj{ch}"):
            for i in offsets:
                wait_for(sd_recv.at[ch, i - 1], xs.at[from_chip(i), ch, other])
                project_chunk(from_chip(i), ch)
    for k in range(X):
        wait_for(q_recv.at[0, k], qall.at[0, streams(k), most])
    for j in order:
        with scope(f"attend0{j}"):
            attend(0, j)
    with scope("proj_rest"):
        for i in offsets:
            project_chip(1, from_chip(i))
    for copy in [*load_o, load_q[1], *load_late, load_m[2]]:
        copy.wait()
    for i in range(NS + 2):
        if i < NS:
            with scope(f"combine0{i}"):
                combine(0, order[i])
        if i >= 2:
            with scope(f"query{i - 2}"):
                next_queries(order[i - 2])
        if i >= 4:
            with scope(f"relay{i - 4}"):
                relay(order[i - 4])
        if i < NS:
            with scope(f"spread0{i}"):
                spread(0, order[i])
        if 1 <= i <= NS:
            with scope(f"settle0{i - 1}"):
                settle(0, order[i - 1], attend_gain[1:2])
    for a in range(NS):
        for i in range(NS - 2 + a, min(NS, NS - 1 + a)):
            with scope(f"relay{i}"):
                relay(order[i])
        with scope(f"attend1{a}"):
            await_queries(order[a])
            attend(1, order[a])
    pads = ((gpad, wgt), (upad, wut))

    def halo_out(number):
        return remote(
            hs.at[number],
            hr.at[number],
            sent.at[11 + number],
            h_recv.at[number],
            "sp",
            lax.rem(s + 1, S),
        )

    def lift(k):
        for h in range(SUB):
            await_rows(2, k * SUB + h, k * SUB + h)
        mixed = xt[2, streams(k)].reshape(SUB * H, D)
        for number, (pad, weight) in enumerate(pads):
            lifted = mm(mixed, weight[...]).astype(BF).astype(F32)
            if k == X - 1:
                hs[number] = lifted[SUB * H - 8 :]

                @pl.when(s < S - 1)
                def _():
                    halo_out(number).start()

            for piece in range(2 * SUB):
                part, core = divmod(piece, 2)
                start = 8 + (2 * k + core) * Rt + part * Rh
                pad[start : start + Rh] = lifted[piece * Rh : (piece + 1) * Rh]

    lifts = [*reversed(range(X))]
    for i in range(NS + 1):
        if i < NS:
            with scope(f"combine1{i}"):
                combine(1, order[i])
            with scope(f"spread1{i}"):
                spread(1, order[i])
            if i > SUB and (i - 1) % SUB == 0:
                with scope(f"lift{i}"):
                    lift(lifts.pop(0))
        if i >= 1:
            with scope(f"settle1{i - 1}"):
                settle(1, order[i - 1], mixer_gain[...])
    with scope("lift"):
        for k in lifts:
            lift(k)

    def hidden_rows(start, stop):
        def convolved(pad, taps):
            return (
                taps[0:1] * pad[6 + start : 6 + stop]
                + taps[1:2] * pad[7 + start : 7 + stop]
                + taps[2:3] * pad[8 + start : 8 + stop]
            )

        gate = convolved(gpad, gate_taps)
        hid[start:stop] = (gate / (1.0 + jnp.exp(-gate)) * convolved(upad, up_taps)).astype(BF)

    with scope("hidden"):
        hidden_rows(16, T)

    @pl.when(s == 0)
    def _():
        for pad, _weight in pads:
            pad[:8] = jnp.zeros((8, F), F32)

    @pl.when(s > 0)
    def _():
        for number, (pad, _weight) in enumerate(pads):
            halo_out(number).wait_recv()
            pad[:8] = hr[number]

    @pl.when(s < S - 1)
    def _():
        for number in range(2):
            halo_out(number).wait_send()

    hidden_rows(0, 16)

    def down_cols(ch):
        return slice(ch * (D // C2), (ch + 1) * (D // C2))

    with scope("down_mm"):
        rows = hid[...]
        for ch in range(C2):
            dpf[:, :, :, down_cols(ch)] = mm(rows, wd[:, down_cols(ch)]).reshape(
                X, 2, Rt, D // C2
            )
            d1s[ch] = dpf[:, other, :, down_cols(ch)].astype(BF)
            remote(d1s.at[ch], d1r.at[ch], sent.at[9], d1_recv.at[ch], "tp", peer).start()
    own = streams(x)
    with scope("down_pair"):
        for ch in range(C2):
            cols = down_cols(ch)
            wait_for(d1_recv.at[ch], d1r.at[ch])
            for i in offsets:
                k = to_chip(i)
                d2s[ch, i - 1] = (dpf[k, c, :, cols] + d1r[ch, k].astype(F32)).astype(BF)
                remote(
                    d2s.at[ch, i - 1],
                    d2r.at[ch, i - 1],
                    sent.at[10],
                    d2_recv.at[ch, i - 1],
                    "tp",
                    k * 2 + c,
                ).start()
            added = dpf[x, c, :, cols] + d1r[ch, x].astype(F32)
            residual[own, :, cols] = residual[own, :, cols] + added.reshape(SUB, Rh, D // C2)
    with scope("drain"):
        first = pl.ds(0, X - 1)
        wait_sent(0, traw.at[first])
        wait_sent(1, xt.at[:, :, 0])
        wait_sent(2, xs.at[first, :, 0])
        wait_sent(3, xs.at[:, :, 0])
        wait_sent(4, qall.at[:, :, most])
        wait_sent(5, osend.at[:, :, most])
        wait_sent(6, ssend.at[:, :, most])
        wait_sent(7, p1s)
        wait_sent(8, p2r)
        wait_sent(9, d1s)
    with scope("down_far"):
        for ch in range(C2):
            cols = down_cols(ch)
            for i in offsets:
                wait_for(d2_recv.at[ch, i - 1], d2r.at[ch, i - 1])
                added = d2r[ch, i - 1].astype(F32)
                residual[own, :, cols] = residual[own, :, cols] + added.reshape(SUB, Rh, D // C2)
    result[...] = normed_rows(residual[own].reshape(Rt, D), final_gain[...]).astype(BF)
    wait_sent(10, d2s)


def body(n, S, *arrays):
    (
        source,
        target,
        source_gain,
        attend_gain,
        query_weight,
        key_weight,
        value_weight,
        out_weight,
        mixer_gain,
        gate_weight,
        up_weight,
        gate_taps,
        up_taps,
        down_weight,
        final_gain,
    ) = arrays
    Rs, D = source.shape
    Rt = target.shape[0]
    W = query_weight.shape[2]
    F = gate_weight.shape[1]
    T = n * Rt
    X = n // 2
    SUB = STREAMS_PER_CHIP
    NS = SUB * X
    Rh = Rt // SUB
    H = 2 * Rh
    NC = SOURCE_CHUNKS
    C = OUT_CHUNKS
    C2 = DOWN_CHUNKS
    RC = Rs // NC
    hbm = pl.BlockSpec(memory_space=pl.ANY)
    dma = pltpu.SemaphoreType.DMA
    scratch = [
        pltpu.VMEM((1, D), F32),
        pltpu.VMEM((2, D), F32),
        pltpu.VMEM((1, D), F32),
        pltpu.VMEM((1, D), F32),
        pltpu.VMEM((3, F), F32),
        pltpu.VMEM((3, F), F32),
        pltpu.VMEM((Rs, D), BF),
        pltpu.VMEM((X, Rt, D), BF),
        pltpu.VMEM((2, D, W), BF),
        pltpu.VMEM((4, D, W), BF),
        pltpu.VMEM((2, W, D), BF),
        pltpu.VMEM((F, D), BF),
        pltpu.VMEM((F, D), BF),
        pltpu.VMEM((D, F), BF),
        pltpu.VMEM((D, F), BF),
        pltpu.VMEM((F, D), BF),
        pltpu.VMEM((X, NC, 2, RC, D), BF),
        pltpu.VMEM((3, NS, 2, Rh, D), BF),
        pltpu.VMEM((4, X, NC, 2 * RC, W), BF),
        pltpu.VMEM((2, NS, S, H, W), BF),
        pltpu.VMEM((2, NS, S, H, W), BF),
        pltpu.VMEM((2, NS, S, H, W), BF),
        pltpu.VMEM((2, NS, S, STAT_ROWS, H), F32),
        pltpu.VMEM((2, NS, S, STAT_ROWS, H), F32),
        pltpu.VMEM((NS, 2, Rh, D), F32),
        pltpu.VMEM((NS, H, W), BF),
        pltpu.VMEM((2, NS, C, Rh, D // C), BF),
        pltpu.VMEM((2, NS, C, Rh, D // C), BF),
        pltpu.VMEM((2, NS, C, Rh, D // C), BF),
        pltpu.VMEM((2, NS, C, X - 1, Rh, D // C), BF),
        pltpu.VMEM((X, 2, Rt, D), F32),
        pltpu.VMEM((C2, X, Rt, D // C2), BF),
        pltpu.VMEM((C2, X, Rt, D // C2), BF),
        pltpu.VMEM((C2, X - 1, Rt, D // C2), BF),
        pltpu.VMEM((C2, X - 1, Rt, D // C2), BF),
        pltpu.VMEM((2, 8, F), F32),
        pltpu.VMEM((2, 8, F), F32),
        pltpu.VMEM((T + 8, F), F32),
        pltpu.VMEM((T + 8, F), F32),
        pltpu.VMEM((T, F), BF),
        pltpu.VMEM((NS, Rh, D), F32),
        dma((12,)),
        dma((13,)),
        dma((X - 1,)),
        dma((3, NS)),
        dma((NC, X - 1)),
        dma((NC, X - 1)),
        dma((1,)),
        dma((2, NS)),
        dma((NS,)),
        dma((2, NS)),
        dma((2, NS)),
        dma((2, NS, C)),
        dma((2, NS, C, X - 1)),
        dma((C2,)),
        dma((C2, X - 1)),
        dma((2,)),
    ]
    return pl.pallas_call(
        functools.partial(kernel, n, S),
        out_shape=pltpu.VMEM((Rt, D), BF),
        in_specs=[hbm] * 15,
        out_specs=pl.BlockSpec(memory_space=pltpu.VMEM),
        scratch_shapes=scratch,
        compiler_params=pltpu.CompilerParams(
            collective_id=0, has_side_effects=True, vmem_limit_bytes=66000000
        ),
    )(
        source,
        target,
        source_gain.reshape(1, D),
        attend_gain,
        query_weight,
        key_weight,
        value_weight,
        out_weight,
        mixer_gain.reshape(1, D),
        gate_weight.T,
        up_weight.T,
        gate_taps,
        up_taps,
        down_weight,
        final_gain.reshape(1, D),
    )


def solution(mesh):
    placed = (
        P(("grp", "sp", "tp"), None),
        P(("grp", "sp", "tp"), None),
        P(),
        P(),
        P(None, None, "tp"),
        P(None, None, "tp"),
        P(None, None, "tp"),
        P(None, "tp", None),
        P(),
        P(None, "tp"),
        P(None, "tp"),
        P(None, "tp"),
        P(None, "tp"),
        P("tp", None),
        P(),
    )
    return jax.shard_map(
        functools.partial(body, mesh.shape["tp"], mesh.shape["sp"]),
        mesh=mesh,
        in_specs=placed,
        out_specs=P(("grp", "sp", "tp"), None),
        check_vma=False,
    )
```

time: 84.2 us -> 79.6 us (0.945)
  Pallas kernels: 83.4 us -> 78.8 us
    pallas_call x1, Pallas kernels: 83.4 us -> 78.8 us  [body(): pl.pallas_call(functools.partial(kernel, n, S), out_shape=pltpu.VMEM((Rt,...]
where the time goes in v3:
time: 79.6 us; the launch traced here: 79.5 us
  Pallas kernels  78.8 us (99%)
    pallas_call x1, Pallas kernels, body(): pl.pallas_call(functools.partial(kernel, n, S), out_shape=pltpu.VMEM((Rt,...  78.8 us

profile of v3, /device:TPU:0, one launch (start us, length us, event | category | flops | bytes accessed | tf_op | source)
XLA Modules:
  0.0 79.5 jit_solution(11751060964149014821)
XLA Ops:
  0.0 78.8 %shard_map.145 = bf16[32,2048]{1,0:T(8,128)(2,1)S(1)} custom-call(bf16[128,2048]{1,0:T(8,128)(2,1)} %source.1, bf16[32,2048]{1,0:T(8,128)(2,1)} %target.1, f32[1,2048]{1,0:T(1,128)} %bitcast.7, f32[2,2048]{1,0:T(2,128)} %attend_gain_in.1, bf16[2,2048,512]{2,1,0:T(8,128)(2,1)} %query_weight.1, bf16[2,2048,512]{2,1,0:T(8,128)(2,1)} %key_weight.1, ...), custom_call_target="tpu_custom_call" | custom-call | tf_op jit(solution)/shard_map/pallas_call | solution.py:719
  78.8 0.7 copy.17

commit v4 on v3

--- a/solution.py
+++ b/solution.py
@@ -9,10 +9,31 @@
 
 HD = 256
 EPS = 1e-06
-STAT_ROWS = 8
 LANES = 128
 SOURCE_CHUNKS = 4
 STREAMS_PER_CHIP = 2
+RELAYED = (2,)
+EARLY = 1
+STEPS = (
+    "a1",
+    "r2",
+    "c0",
+    "a2",
+    "s0",
+    "a3",
+    "c1",
+    "s1",
+    "e0",
+    "c2",
+    "s2",
+    "e1",
+    "c3",
+    "s3",
+    "l0",
+    "e2",
+    "e3",
+    "l1",
+)
 OUT_CHUNKS = 2
 DOWN_CHUNKS = 4
 GROUP_ROWS = 256
@@ -207,11 +228,11 @@
 
     def share_rows(a, rows, number):
         remote(
-            xt.at[a, rows, c], xt.at[a, rows, c], sent.at[1], n_recv.at[a, number], "tp", peer
+            xt.at[a, rows, c], xt.at[a, rows, c], sent.at[1], n_recv.at[number], "tp", peer
         ).start()
 
     def await_rows(a, rows, number):
-        wait_for(n_recv.at[a, number], xt.at[a, rows, other])
+        wait_for(n_recv.at[number], xt.at[a, rows, other])
 
     def first_rows(k):
         rows = traw[k].astype(F32)
@@ -225,35 +246,38 @@
         qall[0, streams(k), s] = mm(rows, wq[0]).astype(BF).reshape(SUB, H, W)
         for block in far_blocks:
             mine = qall.at[0, streams(k), s]
-            remote(mine, mine, sent.at[4], q_recv.at[0, k], "sp", block).start()
+            remote(mine, mine, sent.at[4], q_recv.at[k], "sp", block).start()
 
     def next_queries(j):
         await_rows(1, j, j)
         qall[1, j, s] = mm(xt[1, j].reshape(H, D), wq[1]).astype(BF)
-        if RELAY:
+        if relayed(j):
             mine = qall.at[1, j, s]
             remote(mine, mine, sent.at[4], cross_recv.at[j], "sp", lax.rem(s + half, S)).start()
             to_mates(j, s)
         else:
             for block in far_blocks:
                 mine = qall.at[1, j, s]
-                remote(mine, mine, sent.at[4], q_recv.at[1, j], "sp", block).start()
+                remote(mine, mine, sent.at[4], q_recv.at[j], "sp", block).start()
 
     def to_mates(j, block):
         for m in range(1, half):
             mate = lax.div(s, half) * half + lax.rem(s + m, half)
             rows = qall.at[1, j, block]
-            remote(rows, rows, sent.at[4], q_recv.at[1, j], "sp", mate).start()
+            remote(rows, rows, sent.at[4], q_recv.at[j], "sp", mate).start()
+
+    def relayed(j):
+        return RELAY and order.index(j) in RELAYED
 
     def relay(j):
-        if RELAY:
+        if relayed(j):
             block = lax.rem(s + half, S)
             wait_for(cross_recv.at[j], qall.at[1, j, block])
             to_mates(j, block)
 
     def await_queries(j):
-        count = 2 * (half - 1) if RELAY else S - 1
-        wait_for(q_recv.at[1, j], qall.at[1, j, pl.ds(0, count)])
+        count = 2 * (half - 1) if relayed(j) else S - 1
+        wait_for(q_recv.at[j], qall.at[1, j, pl.ds(0, count)])
 
     def project_chip(layer, k):
         rows = xs[k].reshape(2 * Rs, D)
@@ -301,9 +325,11 @@
                 )
                 packed = jnp.where(lanes == 2 * h, top, packed)
                 packed = jnp.where(lanes == 2 * h + 1, total, packed)
-            stats = packed.T[:STAT_ROWS]
+            stats = packed.T[: 2 * heads]
             for b in range(G):
-                ssend[layer, j, base + b] = stats[:, b * H : (b + 1) * H]
+                ssend[layer, j, base + b] = jnp.concatenate(
+                    [stats[r : r + 1, b * H : (b + 1) * H] for r in range(2 * heads)], axis=1
+                )
 
         if G == S:
             group(0)
@@ -323,7 +349,7 @@
                     src.at[layer, j, block],
                     dst.at[layer, j, s],
                     sent.at[number],
-                    sem.at[layer, j],
+                    sem.at[j],
                     "sp",
                     block,
                 ).start()
@@ -331,21 +357,22 @@
         srecv[layer, j, s] = ssend[layer, j, s]
 
     def combine(layer, j):
-        wait_for(s_recv.at[layer, j], srecv.at[layer, j, most])
-        wait_for(r_recv.at[layer, j], orecv.at[layer, j, most])
-        rows = srecv[layer, j].reshape(S * STAT_ROWS, H)
-        if S * STAT_ROWS < LANES:
-            rows = jnp.concatenate([rows, jnp.zeros((LANES - S * STAT_ROWS, H), F32)], axis=0)
-        stats = rows.T
+        wait_for(s_recv.at[j], srecv.at[layer, j, most])
+        wait_for(r_recv.at[j], orecv.at[layer, j, most])
+        rows = [srecv[layer, j, b] for b in range(S)]
+        room = -S % LANES
+        stats = jnp.concatenate([*rows, jnp.zeros((room, 2 * heads * H), F32)], axis=0).T
         for h in range(heads):
             cols = slice(h * HD, (h + 1) * HD)
-            tops = [stats[:, b * STAT_ROWS + 2 * h :][:, :1] for b in range(S)]
+            top_rows = stats[2 * h * H : (2 * h + 1) * H]
+            total_rows = stats[(2 * h + 1) * H : (2 * h + 2) * H]
+            tops = [top_rows[:, b : b + 1] for b in range(S)]
             highest = functools.reduce(jnp.maximum, tops)
             total = jnp.zeros((H, 1), F32)
             summed = jnp.zeros((H, HD), F32)
             for b in range(S):
                 factor = jnp.exp(tops[b] - highest)
-                total = total + factor * stats[:, b * STAT_ROWS + 2 * h + 1 :][:, :1]
+                total = total + factor * total_rows[:, b : b + 1]
                 summed = summed + factor * orecv[layer, j, b, :, cols].astype(F32)
             att[j, :, cols] = (summed / total).astype(BF)
         rows = att[j]
@@ -357,7 +384,7 @@
                 p1s.at[layer, j, ch],
                 p1r.at[layer, j, ch],
                 sent.at[7],
-                p1_recv.at[layer, j, ch],
+                p1_recv.at[j, ch],
                 "tp",
                 peer,
             ).start()
@@ -365,7 +392,7 @@
     def spread(layer, j):
         for ch in range(C):
             cols = slice(ch * (D // C), (ch + 1) * (D // C))
-            wait_for(p1_recv.at[layer, j, ch], p1r.at[layer, j, ch])
+            wait_for(p1_recv.at[j, ch], p1r.at[layer, j, ch])
             chip_sum = pf[j, c, :, cols] + p1r[layer, j, ch].astype(F32)
             p2s[layer, j, ch] = chip_sum.astype(BF)
             for i in offsets:
@@ -373,7 +400,7 @@
                     p2s.at[layer, j, ch],
                     p2r.at[layer, j, ch, i - 1],
                     sent.at[8],
-                    p2_recv.at[layer, j, ch, i - 1],
+                    p2_recv.at[j, ch, i - 1],
                     "tp",
                     to_chip(i) * 2 + c,
                 ).start()
@@ -383,7 +410,7 @@
         for ch in range(C):
             cols = slice(ch * (D // C), (ch + 1) * (D // C))
             for i in offsets:
-                wait_for(p2_recv.at[layer, j, ch, i - 1], p2r.at[layer, j, ch, i - 1])
+                wait_for(p2_recv.at[j, ch, i - 1], p2r.at[layer, j, ch, i - 1])
                 residual[j, :, cols] = residual[j, :, cols] + p2r[layer, j, ch, i - 1].astype(F32)
         xt[layer + 1, j, c] = normed_rows(residual[j], gain).astype(BF)
         share_rows(layer + 1, j, j)
@@ -460,7 +487,7 @@
                 wait_for(sd_recv.at[ch, i - 1], xs.at[from_chip(i), ch, other])
                 project_chunk(from_chip(i), ch)
     for k in range(X):
-        wait_for(q_recv.at[0, k], qall.at[0, streams(k), most])
+        wait_for(q_recv.at[k], qall.at[0, streams(k), most])
     for j in order:
         with scope(f"attend0{j}"):
             attend(0, j)
@@ -476,22 +503,16 @@
         if i >= 2:
             with scope(f"query{i - 2}"):
                 next_queries(order[i - 2])
-        if i >= 4:
-            with scope(f"relay{i - 4}"):
-                relay(order[i - 4])
+        if EARLY and i == NS:
+            with scope("attend10"):
+                await_queries(order[0])
+                attend(1, order[0])
         if i < NS:
             with scope(f"spread0{i}"):
                 spread(0, order[i])
         if 1 <= i <= NS:
             with scope(f"settle0{i - 1}"):
                 settle(0, order[i - 1], attend_gain[1:2])
-    for a in range(NS):
-        for i in range(NS - 2 + a, min(NS, NS - 1 + a)):
-            with scope(f"relay{i}"):
-                relay(order[i])
-        with scope(f"attend1{a}"):
-            await_queries(order[a])
-            attend(1, order[a])
     pads = ((gpad, wgt), (upad, wut))
 
     def halo_out(number):
@@ -523,21 +544,32 @@
                 pad[start : start + Rh] = lifted[piece * Rh : (piece + 1) * Rh]
 
     lifts = [*reversed(range(X))]
-    for i in range(NS + 1):
-        if i < NS:
-            with scope(f"combine1{i}"):
+
+    def step(name):
+        kind, i = name[0], int(name[1:])
+        with scope(name):
+            if kind == "r":
+                relay(order[i])
+            elif kind == "a":
+                await_queries(order[i])
+                attend(1, order[i])
+            elif kind == "c":
                 combine(1, order[i])
-            with scope(f"spread1{i}"):
+            elif kind == "s":
                 spread(1, order[i])
-            if i > SUB and (i - 1) % SUB == 0:
-                with scope(f"lift{i}"):
-                    lift(lifts.pop(0))
-        if i >= 1:
-            with scope(f"settle1{i - 1}"):
-                settle(1, order[i - 1], mixer_gain[...])
-    with scope("lift"):
-        for k in lifts:
-            lift(k)
+            elif kind == "e":
+                settle(1, order[i], mixer_gain[...])
+            else:
+                lift(lifts[i])
+
+    if NS == 4:
+        steps = STEPS
+    else:
+        steps = [f"r{i}" for i in range(NS)] + [f"a{i}" for i in range(EARLY, NS)]
+        steps += [f"{kind}{i}" for i in range(NS) for kind in "cse"]
+        steps += [f"l{i}" for i in range(X)]
+    for name in steps:
+        step(name)
 
     def hidden_rows(start, stop):
         def convolved(pad, taps):
@@ -680,8 +712,8 @@
         pltpu.VMEM((2, NS, S, H, W), BF),
         pltpu.VMEM((2, NS, S, H, W), BF),
         pltpu.VMEM((2, NS, S, H, W), BF),
-        pltpu.VMEM((2, NS, S, STAT_ROWS, H), F32),
-        pltpu.VMEM((2, NS, S, STAT_ROWS, H), F32),
+        pltpu.VMEM((2, NS, S, 1, 2 * (W // HD) * H), F32),
+        pltpu.VMEM((2, NS, S, 1, 2 * (W // HD) * H), F32),
         pltpu.VMEM((NS, 2, Rh, D), F32),
         pltpu.VMEM((NS, H, W), BF),
         pltpu.VMEM((2, NS, C, Rh, D // C), BF),
@@ -702,16 +734,16 @@
         dma((12,)),
         dma((13,)),
         dma((X - 1,)),
-        dma((3, NS)),
+        dma((NS,)),
         dma((NC, X - 1)),
         dma((NC, X - 1)),
         dma((1,)),
-        dma((2, NS)),
         dma((NS,)),
-        dma((2, NS)),
-        dma((2, NS)),
-        dma((2, NS, C)),
-        dma((2, NS, C, X - 1)),
+        dma((NS,)),
+        dma((NS,)),
+        dma((NS,)),
+        dma((NS, C)),
+        dma((NS, C, X - 1)),
         dma((C2,)),
         dma((C2, X - 1)),
         dma((2,)),

time: 79.6 us -> 77.5 us (0.974)
  Pallas kernels: 78.8 us -> 76.7 us
    pallas_call x1, Pallas kernels: 78.8 us -> 76.7 us  [body(): pl.pallas_call(functools.partial(kernel, n, S), out_shape=pltpu.VMEM((Rt,...]
where the time goes in v4:
time: 77.5 us; the launch traced here: 77.4 us
  Pallas kernels  76.7 us (99%)
    pallas_call x1, Pallas kernels, body(): pl.pallas_call(functools.partial(kernel, n, S), out_shape=pltpu.VMEM((Rt,...  76.7 us

profile of v4, /device:TPU:0, one launch (start us, length us, event | category | flops | bytes accessed | tf_op | source)
XLA Modules:
  0.0 77.4 jit_solution(15647543338675658926)
XLA Ops:
  0.0 76.7 %shard_map.145 = bf16[32,2048]{1,0:T(8,128)(2,1)S(1)} custom-call(bf16[128,2048]{1,0:T(8,128)(2,1)} %source.1, bf16[32,2048]{1,0:T(8,128)(2,1)} %target.1, f32[1,2048]{1,0:T(1,128)} %bitcast.7, f32[2,2048]{1,0:T(2,128)} %attend_gain_in.1, bf16[2,2048,512]{2,1,0:T(8,128)(2,1)} %query_weight.1, bf16[2,2048,512]{2,1,0:T(8,128)(2,1)} %key_weight.1, ...), custom_call_target="tpu_custom_call" | custom-call | tf_op jit(solution)/shard_map/pallas_call | solution.py:751
  76.7 0.7 copy.17

commit v5 on v4

--- a/solution.py
+++ b/solution.py
@@ -12,11 +12,12 @@
 LANES = 128
 SOURCE_CHUNKS = 4
 STREAMS_PER_CHIP = 2
-RELAYED = (2,)
-EARLY = 1
+RELAYED = (1, 2)
 STEPS = (
+    "r1",
+    "a0",
+    "r2",
     "a1",
-    "r2",
     "c0",
     "a2",
     "s0",
@@ -36,6 +37,8 @@
 )
 OUT_CHUNKS = 2
 DOWN_CHUNKS = 4
+RAW = 1
+DOWN_RAW = 1
 GROUP_ROWS = 256
 MESH = pl.DeviceIdType.MESH
 BF = jnp.bfloat16
@@ -103,11 +106,13 @@
     p1r,
     p2s,
     p2r,
+    rr,
     dpf,
     d1s,
     d1r,
     d2s,
     d2r,
+    rd,
     hs,
     hr,
     gpad,
@@ -127,8 +132,10 @@
     s_recv,
     p1_recv,
     p2_recv,
+    rr_recv,
     d1_recv,
     d2_recv,
+    rd_recv,
     h_recv,
 ):
     X = n // 2
@@ -197,6 +204,9 @@
     for i in offsets:
         pl.semaphore_signal(
             barrier, inc=1, device_id={"tp": to_chip(i) * 2 + c}, device_id_type=MESH
+        )
+        pl.semaphore_signal(
+            barrier, inc=1, device_id={"tp": to_chip(i) * 2 + other}, device_id_type=MESH
         )
     for block in far_blocks:
         pl.semaphore_signal(barrier, inc=1, device_id={"sp": block}, device_id_type=MESH)
@@ -388,22 +398,38 @@
                 "tp",
                 peer,
             ).start()
+            if ch < RAW:
+                p2s[layer, j, ch] = pf[j, c, :, cols].astype(BF)
+                for i in offsets:
+                    chip_copy(layer, j, ch, i).start()
+                    remote(
+                        p1s.at[layer, j, ch],
+                        rr.at[layer, j, ch, i - 1],
+                        sent.at[13],
+                        rr_recv.at[j, ch, i - 1],
+                        "tp",
+                        to_chip(i) * 2 + other,
+                    ).start()
+
+    def chip_copy(layer, j, ch, i):
+        return remote(
+            p2s.at[layer, j, ch],
+            p2r.at[layer, j, ch, i - 1],
+            sent.at[8],
+            p2_recv.at[j, ch, i - 1],
+            "tp",
+            to_chip(i) * 2 + c,
+        )
 
     def spread(layer, j):
         for ch in range(C):
             cols = slice(ch * (D // C), (ch + 1) * (D // C))
             wait_for(p1_recv.at[j, ch], p1r.at[layer, j, ch])
             chip_sum = pf[j, c, :, cols] + p1r[layer, j, ch].astype(F32)
-            p2s[layer, j, ch] = chip_sum.astype(BF)
-            for i in offsets:
-                remote(
-                    p2s.at[layer, j, ch],
-                    p2r.at[layer, j, ch, i - 1],
-                    sent.at[8],
-                    p2_recv.at[j, ch, i - 1],
-                    "tp",
-                    to_chip(i) * 2 + c,
-                ).start()
+            if ch >= RAW:
+                p2s[layer, j, ch] = chip_sum.astype(BF)
+                for i in offsets:
+                    chip_copy(layer, j, ch, i).start()
             residual[j, :, cols] = residual[j, :, cols] + chip_sum
 
     def settle(layer, j, gain):
@@ -412,6 +438,11 @@
             for i in offsets:
                 wait_for(p2_recv.at[j, ch, i - 1], p2r.at[layer, j, ch, i - 1])
                 residual[j, :, cols] = residual[j, :, cols] + p2r[layer, j, ch, i - 1].astype(F32)
+                if ch < RAW:
+                    wait_for(rr_recv.at[j, ch, i - 1], rr.at[layer, j, ch, i - 1])
+                    residual[j, :, cols] = residual[j, :, cols] + rr[
+                        layer, j, ch, i - 1
+                    ].astype(F32)
         xt[layer + 1, j, c] = normed_rows(residual[j], gain).astype(BF)
         share_rows(layer + 1, j, j)
 
@@ -424,7 +455,7 @@
         lax.fori_loop(0, D // GROUP_ROWS, one, 0)
 
     with scope("barrier"):
-        pl.semaphore_wait(barrier, X + S - 1)
+        pl.semaphore_wait(barrier, 2 * X - 1 + S - 1)
     load_t.wait()
     for i in offsets:
         remote(
@@ -503,10 +534,6 @@
         if i >= 2:
             with scope(f"query{i - 2}"):
                 next_queries(order[i - 2])
-        if EARLY and i == NS:
-            with scope("attend10"):
-                await_queries(order[0])
-                attend(1, order[0])
         if i < NS:
             with scope(f"spread0{i}"):
                 spread(0, order[i])
@@ -565,7 +592,7 @@
     if NS == 4:
         steps = STEPS
     else:
-        steps = [f"r{i}" for i in range(NS)] + [f"a{i}" for i in range(EARLY, NS)]
+        steps = [f"r{i}" for i in range(NS)] + [f"a{i}" for i in range(NS)]
         steps += [f"{kind}{i}" for i in range(NS) for kind in "cse"]
         steps += [f"l{i}" for i in range(X)]
     for name in steps:
@@ -605,6 +632,16 @@
 
     def down_cols(ch):
         return slice(ch * (D // C2), (ch + 1) * (D // C2))
+
+    def down_chip(ch, i):
+        return remote(
+            d2s.at[ch, i - 1],
+            d2r.at[ch, i - 1],
+            sent.at[10],
+            d2_recv.at[ch, i - 1],
+            "tp",
+            to_chip(i) * 2 + c,
+        )
 
     with scope("down_mm"):
         rows = hid[...]
@@ -614,6 +651,19 @@
             )
             d1s[ch] = dpf[:, other, :, down_cols(ch)].astype(BF)
             remote(d1s.at[ch], d1r.at[ch], sent.at[9], d1_recv.at[ch], "tp", peer).start()
+            if ch < DOWN_RAW:
+                for i in offsets:
+                    k = to_chip(i)
+                    d2s[ch, i - 1] = dpf[k, c, :, down_cols(ch)].astype(BF)
+                    down_chip(ch, i).start()
+                    remote(
+                        d1s.at[ch, k],
+                        rd.at[ch, i - 1],
+                        sent.at[14],
+                        rd_recv.at[ch, i - 1],
+                        "tp",
+                        k * 2 + other,
+                    ).start()
     own = streams(x)
     with scope("down_pair"):
         for ch in range(C2):
@@ -621,15 +671,9 @@
             wait_for(d1_recv.at[ch], d1r.at[ch])
             for i in offsets:
                 k = to_chip(i)
-                d2s[ch, i - 1] = (dpf[k, c, :, cols] + d1r[ch, k].astype(F32)).astype(BF)
-                remote(
-                    d2s.at[ch, i - 1],
-                    d2r.at[ch, i - 1],
-                    sent.at[10],
-                    d2_recv.at[ch, i - 1],
-                    "tp",
-                    k * 2 + c,
-                ).start()
+                if ch >= DOWN_RAW:
+                    d2s[ch, i - 1] = (dpf[k, c, :, cols] + d1r[ch, k].astype(F32)).astype(BF)
+                    down_chip(ch, i).start()
             added = dpf[x, c, :, cols] + d1r[ch, x].astype(F32)
             residual[own, :, cols] = residual[own, :, cols] + added.reshape(SUB, Rh, D // C2)
     with scope("drain"):
@@ -644,15 +688,20 @@
         wait_sent(7, p1s)
         wait_sent(8, p2r)
         wait_sent(9, d1s)
+        wait_sent(13, rr)
     with scope("down_far"):
         for ch in range(C2):
             cols = down_cols(ch)
             for i in offsets:
                 wait_for(d2_recv.at[ch, i - 1], d2r.at[ch, i - 1])
                 added = d2r[ch, i - 1].astype(F32)
+                if ch < DOWN_RAW:
+                    wait_for(rd_recv.at[ch, i - 1], rd.at[ch, i - 1])
+                    added = added + rd[ch, i - 1].astype(F32)
                 residual[own, :, cols] = residual[own, :, cols] + added.reshape(SUB, Rh, D // C2)
     result[...] = normed_rows(residual[own].reshape(Rt, D), final_gain[...]).astype(BF)
     wait_sent(10, d2s)
+    wait_sent(14, rd)
 
 
 def body(n, S, *arrays):
@@ -720,11 +769,13 @@
         pltpu.VMEM((2, NS, C, Rh, D // C), BF),
         pltpu.VMEM((2, NS, C, Rh, D // C), BF),
         pltpu.VMEM((2, NS, C, X - 1, Rh, D // C), BF),
+        pltpu.VMEM((2, NS, RAW, X - 1, Rh, D // C), BF),
         pltpu.VMEM((X, 2, Rt, D), F32),
         pltpu.VMEM((C2, X, Rt, D // C2), BF),
         pltpu.VMEM((C2, X, Rt, D // C2), BF),
         pltpu.VMEM((C2, X - 1, Rt, D // C2), BF),
         pltpu.VMEM((C2, X - 1, Rt, D // C2), BF),
+        pltpu.VMEM((DOWN_RAW, X - 1, Rt, D // C2), BF),
         pltpu.VMEM((2, 8, F), F32),
         pltpu.VMEM((2, 8, F), F32),
         pltpu.VMEM((T + 8, F), F32),
@@ -732,7 +783,7 @@
         pltpu.VMEM((T, F), BF),
         pltpu.VMEM((NS, Rh, D), F32),
         dma((12,)),
-        dma((13,)),
+        dma((15,)),
         dma((X - 1,)),
         dma((NS,)),
         dma((NC, X - 1)),
@@ -744,8 +795,10 @@
         dma((NS,)),
         dma((NS, C)),
         dma((NS, C, X - 1)),
+        dma((NS, RAW, X - 1)),
         dma((C2,)),
         dma((C2, X - 1)),
+        dma((DOWN_RAW, X - 1)),
         dma((2,)),
     ]
     return pl.pallas_call(

time: 77.5 us -> 77.5 us (level)
  no operation moved by 1% of the time
where the time goes in v5:
time: 77.5 us; the launch traced here: 77.3 us
  Pallas kernels  76.6 us (99%)
    pallas_call x1, Pallas kernels, body(): pl.pallas_call(functools.partial(kernel, n, S), out_shape=pltpu.VMEM((Rt,...  76.6 us

profile of v5, /device:TPU:0, one launch (start us, length us, event | category | flops | bytes accessed | tf_op | source)
XLA Modules:
  0.0 77.3 jit_solution(3191177783176671500)
XLA Ops:
  0.0 76.6 %shard_map.145 = bf16[32,2048]{1,0:T(8,128)(2,1)S(1)} custom-call(bf16[128,2048]{1,0:T(8,128)(2,1)} %source.1, bf16[32,2048]{1,0:T(8,128)(2,1)} %target.1, f32[1,2048]{1,0:T(1,128)} %bitcast.7, f32[2,2048]{1,0:T(2,128)} %attend_gain_in.1, bf16[2,2048,512]{2,1,0:T(8,128)(2,1)} %query_weight.1, bf16[2,2048,512]{2,1,0:T(8,128)(2,1)} %key_weight.1, ...), custom_call_target="tpu_custom_call" | custom-call | tf_op jit(solution)/shard_map/pallas_call | solution.py:804
  76.7 0.7 copy.17
